TPU v7x, 512 devices: a whole 4x4x16 slice. The times are simulated.
512 devices in a mesh: ep: 32 (over z, core), tp: 16 (over y, x).
Axes of the slice: x: 4, y: 4, z: 16, core: 2. Of those that a mesh axis runs over, the one named last changes fastest.
Arguments:
- q_latent: bfloat16 [16384, 512], P('ep'), may hold values from -6 to 6
- kv_latent: bfloat16 [16384, 256], P('ep'), may hold values from -6 to 6
- rope_key: bfloat16 [16384, 32], P('ep'), may hold values from -400 to 400
- q_gain: bfloat16 [512], replicated, may hold values from 0.099609375 to 1.8984375
- kv_gain: bfloat16 [256], replicated, may hold values from 0.099609375 to 1.8984375
- w_q_nope: bfloat16 [512, 1024], P(None, 'tp'), may hold values from -0.25 to 0.25
- w_q_rope: bfloat16 [512, 512], P(None, 'tp'), may hold values from -0.25 to 0.25
- w_k_nope: bfloat16 [256, 1024], P(None, 'tp'), may hold values from -0.375 to 0.375
- w_value: bfloat16 [256, 1024], P(None, 'tp'), may hold values from -0.375 to 0.375
- w_out: bfloat16 [1024, 2048], P('tp'), may hold values from -5.375 to 5.375
- tokens_b: bfloat16 [4096, 2048], P('ep'), may hold values from -6 to 6
- norm_gain_b: bfloat16 [2048], replicated, may hold values from 0.099609375 to 1.8984375
- routes: int32 [4096, 2], P('ep'), may hold values from 0 to 31, all different within a row; in each aligned block of 128 rows (0 to 127, 128 to 255, ...) at most 12 rows name the same one
- route_logits: float32 [4096, 2], P('ep'), may hold values from -6 to 6
- w_gate: bfloat16 [32, 2048, 4096], P('ep', None, 'tp'), may hold values from -0.125 to 0.125
- w_up: bfloat16 [32, 2048, 4096], P('ep', None, 'tp'), may hold values from -0.125 to 0.125
- w_down: bfloat16 [32, 4096, 2048], P('ep', 'tp'), may hold values from -0.125 to 0.125
Outputs:
- mixer_out: bfloat16 [16384, 2048], P(('ep', 'tp'))
- expert_mix: bfloat16 [4096, 2048], P('ep', 'tp')
Inputs may be any that keep to these rules, and one draw needn't show every extreme that they name: `routes`: each row names two different experts. In each aligned block of 128 rows (the rows of one index of ep) no expert is named by more than 12 rows, and in every draw some expert is named by exactly 12 rows of some block.
All inputs are finite; a program needn't handle non-finite values.
Results may differ from a plain program's by a relative error of at most 0.022.
The roundings to bfloat16 on the way count: a program that leaves them out, or rounds other values in their place, can miss the bound.
Values may be sent and summed in bfloat16 or wider, within the bound.
No kernel may reach another device: no remote copies, remote signals or barrier semaphores. Data moves between devices by JAX's collectives and lax.ppermute only.
A program may use at most 128 MiB of HBM per device.

v0:
```python
import jax
import jax.numpy as jnp
from jax import lax
from jax.sharding import PartitionSpec as P

NOPE = 64
ROPE = 32
VDIM = 64


EPSILON = 1e-06
FLOOR = -1e30


def side_by_side(arrays, axis, dim, along):
    ends, at = ([], 0)
    for a in arrays[:-1]:
        at += a.shape[along]
        ends.append(at)
    both = jnp.concatenate(arrays, axis=along)
    return tuple(jnp.split(lax.all_gather(both, axis, axis=dim, tiled=True), ends, axis=along))


def cut_along(x, dim, count):
    before, after = (x.shape[:dim], x.shape[dim + 1 :])
    return jnp.moveaxis(x.reshape(*before, count, -1, *after), dim, 0)


def sent_and_summed(x, axis, dim):
    pieces = cut_along(x, dim, lax.axis_size(axis))
    arrived = lax.all_to_all(pieces, axis, split_axis=0, concat_axis=0, tiled=True)
    return arrived.astype(jnp.float32).sum(axis=0)


def from_everyone(x, axis):
    copies = jnp.broadcast_to(x, (lax.axis_size(axis), *x.shape))
    return lax.all_to_all(copies, axis, split_axis=0, concat_axis=0, tiled=True)


def in_order(pieces, dim):
    dims = list(pieces.shape[1:])
    dims[dim] *= pieces.shape[0]
    return jnp.moveaxis(pieces, 0, dim).reshape(dims)


def collect(x, axis, dim):
    pieces = from_everyone(x, axis)
    return in_order(pieces, dim)


def rms_rows(values, gain):
    wide = values.astype(jnp.float32)
    scaled = wide * lax.rsqrt(jnp.mean(wide * wide, axis=-1, keepdims=True) + EPSILON)
    return (scaled * gain.astype(jnp.float32)).astype(jnp.bfloat16)


def rotate(values, places):
    half = values.shape[-1] // 2
    freqs = 10000.0 ** (-jnp.arange(half, dtype=jnp.float32) / half)
    angles = places.astype(jnp.float32)[:, None] * freqs[None, :]
    cosine = jnp.cos(angles)[:, None, :]
    sine = jnp.sin(angles)[:, None, :]
    first = values[..., :half]
    second = values[..., half:]
    return jnp.concatenate(
        [first * cosine - second * sine, first * sine + second * cosine], axis=-1
    )


def key_side(kv_piece, rope_piece, kv_gain, w_k_nope, w_value):
    count = kv_piece.shape[0]
    places = jnp.arange(count, dtype=jnp.int32)
    normed = rms_rows(kv_piece, kv_gain)
    k_nope = jnp.dot(normed, w_k_nope, preferred_element_type=jnp.float32).astype(jnp.bfloat16)
    values = jnp.dot(normed, w_value, preferred_element_type=jnp.float32).astype(jnp.bfloat16)
    k_rope = rotate(rope_piece.astype(jnp.float32)[:, None, :], places)[:, 0].astype(jnp.bfloat16)
    return (k_nope, values, k_rope)


def attend_block(carry, q_nope, q_rope, k_nope, values, k_rope):
    top, total_w, acc = carry
    heads = q_nope.shape[1]
    count = k_nope.shape[0]
    key_heads = k_nope.reshape(count, heads, NOPE)
    value_heads = values.reshape(count, heads, VDIM)
    scores = jnp.einsum("qhd,khd->hqk", q_nope, key_heads, preferred_element_type=jnp.float32)
    scores = scores + jnp.einsum("qhr,kr->hqk", q_rope, k_rope, preferred_element_type=jnp.float32)
    scores = scores * (NOPE + ROPE) ** (-0.5)
    new_top = jnp.maximum(top, jnp.max(scores, axis=-1))
    shrink = jnp.exp(top - new_top)
    weights = jnp.exp(scores - new_top[..., None])
    total_w = total_w * shrink + jnp.sum(weights, axis=-1)
    acc = acc * shrink[..., None] + jnp.einsum(
        "hqk,khd->hqd",
        weights.astype(jnp.bfloat16),
        value_heads,
        preferred_element_type=jnp.float32,
    )
    return (new_top, total_w, acc)


def attend(carry, q_nope, q_rope, k_nope, values, k_rope):
    count = k_nope.shape[0]
    span = 512

    def advance(state, pieces):
        return (attend_block(state, q_nope, q_rope, pieces[0], pieces[1], pieces[2]), None)

    blocks = (
        k_nope.reshape(count // span, span, k_nope.shape[1]),
        values.reshape(count // span, span, values.shape[1]),
        k_rope.reshape(count // span, span, k_rope.shape[1]),
    )
    carry, _ = lax.scan(advance, carry, blocks)
    return carry


def shards(
    q_latent,
    kv_latent,
    rope_key,
    q_gain,
    kv_gain,
    w_q_nope,
    w_q_rope,
    w_k_nope,
    w_value,
    w_out,
    tokens_b,
    norm_gain_b,
    routes,
    route_logits,
    w_gate,
    w_up,
    w_down,
):
    own_rows = q_latent.shape[0]
    heads = w_q_nope.shape[1] // NOPE
    offset = lax.axis_index("ep") * own_rows
    places = offset + jnp.arange(own_rows, dtype=jnp.int32)
    q_normed = rms_rows(q_latent, q_gain)
    q_nope = jnp.dot(q_normed, w_q_nope, preferred_element_type=jnp.float32).astype(jnp.bfloat16)
    q_nope = q_nope.reshape(own_rows, heads, NOPE)
    q_turn = jnp.dot(q_normed, w_q_rope, preferred_element_type=jnp.float32).reshape(
        own_rows, heads, ROPE
    )
    q_rope = rotate(q_turn, places).astype(jnp.bfloat16)
    start_carry = (
        jnp.full((heads, own_rows), FLOOR, jnp.float32),
        jnp.zeros((heads, own_rows), jnp.float32),
        jnp.zeros((heads, own_rows, VDIM), jnp.float32),
    )
    pieces = side_by_side((kv_latent, rope_key), "ep", 0, 1)
    piece_keys, piece_values, piece_rotary = key_side(
        pieces[0], pieces[1], kv_gain, w_k_nope, w_value
    )
    top, total_w, acc = attend(start_carry, q_nope, q_rope, piece_keys, piece_values, piece_rotary)
    attended = (acc / total_w[..., None]).astype(jnp.bfloat16)
    attended = attended.transpose(1, 0, 2).reshape(own_rows, heads * VDIM)
    rows = attended
    mixer_out = sent_and_summed(
        jnp.dot(rows, w_out, preferred_element_type=jnp.float32).astype(jnp.bfloat16), "tp", 0
    ).astype(jnp.bfloat16)
    n_ep = lax.axis_size("ep")
    n_tp = lax.axis_size("tp")
    rows_b = tokens_b.shape[0]
    width = tokens_b.shape[1]
    room = 3 * rows_b // n_ep
    normed_b = rms_rows(tokens_b, norm_gain_b)
    weights_b = jax.nn.softmax(route_logits, axis=-1)
    flat = routes.reshape(-1)
    assigned = flat.shape[0]
    onehot = (flat[:, None] == jnp.arange(n_ep, dtype=jnp.int32)[None, :]).astype(jnp.int32)
    slot = jnp.sum((jnp.cumsum(onehot, axis=0) - 1) * onehot, axis=1)
    where = flat * room + slot
    table = (
        jnp.full((n_ep * room,), assigned, jnp.int32)
        .at[where]
        .set(jnp.arange(assigned, dtype=jnp.int32))
    )
    padded = jnp.concatenate([normed_b, jnp.zeros((1, width), jnp.bfloat16)], axis=0)
    share = width // n_tp
    narrow_rows = lax.dynamic_slice_in_dim(padded, lax.axis_index("tp") * share, share, 1)
    outgoing = narrow_rows[table // 2].reshape(n_ep, room, share)
    arrived = lax.all_to_all(outgoing, "ep", split_axis=0, concat_axis=0, tiled=True)
    sources, count, piece_width = arrived.shape
    rows = arrived.reshape(sources * count, piece_width)
    piece = collect(rows, "tp", 1)
    gate_rows = w_gate[0]
    up_rows = w_up[0]
    gate = jnp.dot(piece, gate_rows, preferred_element_type=jnp.float32)
    up = jnp.dot(piece, up_rows, preferred_element_type=jnp.float32)
    hidden = (jax.nn.silu(gate) * up).astype(jnp.bfloat16)
    term = jnp.dot(hidden, w_down[0], preferred_element_type=jnp.float32)
    summed = sent_and_summed(term.astype(jnp.bfloat16), "tp", 1)
    finished = summed.astype(jnp.bfloat16).reshape(sources, count, summed.shape[1])
    back = lax.all_to_all(finished, "ep", split_axis=0, concat_axis=0, tiled=True)
    back = back.reshape(n_ep * room, back.shape[2])
    picked = back[where.reshape(rows_b, 2)].astype(jnp.float32)
    expert_mix = jnp.sum(picked * weights_b[:, :, None], axis=1).astype(jnp.bfloat16)
    return (mixer_out, expert_mix)


def solution(mesh):
    placed = (
        P("ep", None),
        P("ep", None),
        P("ep", None),
        P(),
        P(),
        P(None, "tp"),
        P(None, "tp"),
        P(None, "tp"),
        P(None, "tp"),
        P("tp", None),
        P("ep", None),
        P(),
        P("ep", None),
        P("ep", None),
        P("ep", None, "tp"),
        P("ep", None, "tp"),
        P("ep", "tp", None),
    )
    return jax.shard_map(
        shards,
        mesh=mesh,
        in_specs=placed,
        out_specs=(P(("ep", "tp"), None), P("ep", "tp")),
        check_vma=False,
    )
```

profile of v0, /device:TPU:1, one launch (start us, length us, event | category | flops | bytes accessed | tf_op | source)
XLA Modules:
  0.0 334.1 jit_solution(13218772550835905162)
XLA Ops:
  8.4 1.5 pad_maximum_fusion.1
  13.0 1.4 scatter_custom_fusion
  14.4 1.2 fusion.37
  15.6 1.2 fusion.39
  16.9 1.4 gather_fusion
  18.4 34.7 %all_to_all.25 = bf16[32,12,128]{2,1,0:T(8,128)(2,1)S(1)} all-to-all(bf16[32,12,128]{2,1,0:T(8,128)(2,1)S(1)} %reshape.366), channel_id=1, replica_groups=mesh['ep'=32,'tp'=16] {'ep'}, dimensions={0} | all-to-all | bytes 196608 | tf_op jit(solution)/shard_map/all_to_all | solution.py:185
  53.4 28.2 %all_to_all.26 = bf16[16,384,128]{1,2,0:T(8,128)(2,1)S(1)} all-to-all(bf16[16,384,128]{1,2,0:T(8,128)(2,1)S(1)} %broadcast_in_dim.28), channel_id=1, replica_groups=mesh['ep'=32,'tp'=16] {'tp'}, dimensions={0} | all-to-all | bytes 3145728 | tf_op jit(solution)/shard_map/all_to_all | solution.py:37
  81.6 1.9 fusion.47
  83.5 4.2 %fusion.25 = bf16[48,16,8,128]{3,2,1,0:T(8,128)(2,1)} fusion(bf16[1,256,2048]{2,1,0:T(8,128)(2,1)S(1)} %copy-done, bf16[384,2048]{0,1:T(8,128)(2,1)S(1)} %bitcast.134, bf16[1,2048,256]{2,1,0:T(8,128)(2,1)} %param.34, f32[384,256]{1,0:T(8,128)S(1)} %fusion.47), kind=kOutput, calls=%fused_computation.44 | convolution fusion | flops 806682624 | bytes 5636096 | tf_op jit(solution)/shard_map/dot_general | solution.py:194
  87.8 3.0 copy.52
  90.8 3.7 %all-to-all-start.3 = ((bf16[16,384,128]{2,1,0:T(8,128)(2,1)}), bf16[16,384,128]{2,1,0:T(8,128)(2,1)S(1)}, u32[]{:S(2)}, u32[]{:S(2)}) async-start(bf16[16,384,128]{2,1,0:T(8,128)(2,1)} %bitcast.132), calls=%async_computation.3 | async-start | bytes 3145728 | tf_op jit(solution)/shard_map/all_to_all | solution.py:31
  96.7 18.4 %all-to-all-done.3 = bf16[16,384,128]{2,1,0:T(8,128)(2,1)S(1)} async-done(((bf16[16,384,128]{2,1,0:T(8,128)(2,1)}), bf16[16,384,128]{2,1,0:T(8,128)(2,1)S(1)}, u32[]{:S(2)}, u32[]{:S(2)}) %all-to-all-start.3) | async-done | bytes 1572896 | tf_op jit(solution)/shard_map/all_to_all | solution.py:31
  116.0 10.0 %all-to-all-start.4 = ((bf16[32,12,128]{2,1,0:T(8,128)(2,1)}), bf16[32,12,128]{2,1,0:T(8,128)(2,1)S(1)}, u32[]{:S(2)}, u32[]{:S(2)}) async-start(bf16[32,12,128]{2,1,0:T(8,128)(2,1)} %reshape.370), calls=%async_computation.4 | async-start | bytes 262144 | tf_op jit(solution)/shard_map/all_to_all | solution.py:197
  126.0 5.1 %fusion.22 = f32[16384]{0:T(1024)S(1)} fusion(bf16[16384,288]{0,1:T(8,128)(2,1)} %all-gather.2.cloned.1.call-done), kind=kLoop, calls=%fused_computation.36 | loop fusion | flops 12566528 | bytes 8454144 | tf_op jit(solution)/shard_map/reduce_sum | solution.py:53
  131.1 7.1 %convolution_convert_fusion = bf16[16384,64]{0,1:T(8,128)(2,1)} fusion(bf16[256,64]{0,1:T(8,128)(2,1)S(1)} %copy-done.6, f32[256]{0:T(256)S(1)} %convert_element_type.102, f32[16384]{0:T(1024)S(1)} %add_rsqrt_fusion, bf16[16384,288]{0,1:T(8,128)(2,1)} %all-gather.2.cloned.1.call-done), kind=kOutput, calls=%fused_computation.34 | convolution fusion | flops 554696704 | bytes 10585088 | tf_op jit(solution)/shard_map/dot_general | solution.py:75
  138.3 4.8 %copy.47 = bf16[16384,64]{1,0:T(8,128)(2,1)} copy(bf16[16384,64]{0,1:T(8,128)(2,1)} %convolution_convert_fusion) | data formatting | bytes 4194304
  143.1 7.2 %convolution_convert_fusion.1 = bf16[16384,64]{0,1:T(8,128)(2,1)} fusion(bf16[256,64]{0,1:T(8,128)(2,1)S(1)} %copy-done.7, f32[256]{0:T(256)S(1)} %convert_element_type.102, f32[16384]{0:T(1024)S(1)} %add_rsqrt_fusion, bf16[16384,288]{0,1:T(8,128)(2,1)} %all-gather.2.cloned.1.call-done), kind=kOutput, calls=%fused_computation.35 | convolution fusion | flops 554696704 | bytes 10585088 | tf_op jit(solution)/shard_map/dot_general | solution.py:74
  150.3 4.8 %copy.45 = bf16[16384,64]{1,0:T(8,128)(2,1)} copy(bf16[16384,64]{0,1:T(8,128)(2,1)} %convolution_convert_fusion.1) | data formatting | bytes 4194304
  155.1 1.4 fusion.44
  156.5 4.2 %fusion.41 = (bf16[16384,1,16]{0,2,1:T(8,128)(2,1)S(1)}, bf16[16384,1,16]{0,2,1:T(8,128)(2,1)S(1)}) fusion(f32[16384,1,32]{0,2,1:T(8,128)S(1)} %fusion.44, f32[16]{0:T(128)S(1)} %multiply_power_fusion, f32[16384]{0:T(1024)S(1)} %iota_convert_fusion), kind=kLoop, calls=%fused_computation.65 | loop fusion | flops 2359296 | bytes 3211328 | tf_op jit(solution)/shard_map/convert.5
  160.8 3.1 copy.46
  163.9 123.6 %while.15 = (s32[]{:T(128)}, f32[1,512]{1,0:T(1,128)S(1)}, f32[1,512]{1,0:T(1,128)S(1)}, f32[1,512,64]{1,2,0:T(8,128)S(1)}, bf16[32,512,64]{2,1,0:T(8,128)(2,1)}...) while((s32[]{:T(128)}, f32[1,512]{1,0:T(1,128)S(1)}, ...), condition=%wide.region_5.6_spmd.clone, body=%wide.region_2.5_spmd.clone.sunk | while | flops 85821952 | bytes 6029453 | solution.py:114
  170.4 1.2 fusion.104
  182.0 1.2 fusion.104
  189.7 1.2 fusion.104
  193.6 1.2 fusion.104
  201.3 1.2 fusion.104
  212.9 1.2 fusion.104
  224.5 1.2 fusion.104
  287.5 2.1 convolution_convert_fusion.2
  289.6 3.7 %all-to-all-start = ((bf16[16,32,2048]{2,1,0:T(8,128)(2,1)}), bf16[16,32,2048]{2,1,0:T(8,128)(2,1)S(1)}, u32[]{:S(2)}, u32[]{:S(2)}) async-start(bf16[16,32,2048]{2,1,0:T(8,128)(2,1)} %bitcast.9), calls=%async_computation | async-start | bytes 4194304 | tf_op jit(solution)/shard_map/all_to_all | solution.py:31
  295.4 30.8 %all-to-all-done = bf16[16,32,2048]{2,1,0:T(8,128)(2,1)S(1)} async-done(((bf16[16,32,2048]{2,1,0:T(8,128)(2,1)}), bf16[16,32,2048]{2,1,0:T(8,128)(2,1)S(1)}, u32[]{:S(2)}, u32[]{:S(2)}) %all-to-all-start) | async-done | bytes 2097184 | tf_op jit(solution)/shard_map/all_to_all | solution.py:31
  (291 shorter events, 124.3 us)
Async XLA Ops:
  7.2 76.3 %copy-start = (bf16[1,256,2048]{2,1,0:T(8,128)(2,1)S(1)}, bf16[1,256,2048]{2,1,0:T(8,128)(2,1)}, u32[]{:S(2)}) copy-start(bf16[1,256,2048]{2,1,0:T(8,128)(2,1)} %param.35) | copy-start | bytes 3145732
  7.2 118.8 %all-gather.2.cloned.1.call-start = ((), (), s32[]{:S(2)}) async-start(), calls=%async_computation.5 | async-start | bytes 9732096 | tf_op jit(solution)/shard_map/all_gather | solution.py:21
  87.8 6.8 %copy-start.8 = (bf16[256]{0:T(256)(128)(2,1)S(1)}, bf16[256]{0:T(256)(128)(2,1)}, u32[]{:S(2)}) copy-start(bf16[256]{0:T(256)(128)(2,1)} %param.23) | copy-start | bytes 1540
  87.8 6.8 %copy-start.4 = (bf16[512]{0:T(512)(128)(2,1)S(1)}, bf16[512]{0:T(512)(128)(2,1)}, u32[]{:S(2)}) copy-start(bf16[512]{0:T(512)(128)(2,1)} %param.22) | copy-start | bytes 3076
  87.8 6.9 %copy-start.1 = (bf16[512,512]{1,0:T(8,128)(2,1)S(1)}, bf16[512,512]{1,0:T(8,128)(2,1)}, u32[]{:S(2)}) copy-start(bf16[512,512]{1,0:T(8,128)(2,1)} %param.19) | copy-start | bytes 1572868
  87.8 7.1 %copy-start.5 = (bf16[512,32]{0,1:T(8,128)(2,1)S(1)}, bf16[512,32]{0,1:T(8,128)(2,1)}, u32[]{:S(2)}) copy-start(bf16[512,32]{0,1:T(8,128)(2,1)} %param.25) | copy-start | bytes 98308
  90.8 24.3 %all-to-all-start.3 = ((bf16[16,384,128]{2,1,0:T(8,128)(2,1)}), bf16[16,384,128]{2,1,0:T(8,128)(2,1)S(1)}, u32[]{:S(2)}, u32[]{:S(2)}) async-start(bf16[16,384,128]{2,1,0:T(8,128)(2,1)} %bitcast.132), calls=%async_computation.3 | async-start | bytes 3145728 | tf_op jit(solution)/shard_map/all_to_all | solution.py:31
  116.0 173.6 %all-to-all-start.4 = ((bf16[32,12,128]{2,1,0:T(8,128)(2,1)}), bf16[32,12,128]{2,1,0:T(8,128)(2,1)S(1)}, u32[]{:S(2)}, u32[]{:S(2)}) async-start(bf16[32,12,128]{2,1,0:T(8,128)(2,1)} %reshape.370), calls=%async_computation.4 | async-start | bytes 262144 | tf_op jit(solution)/shard_map/all_to_all | solution.py:197
  125.9 5.2 %copy-start.6 = (bf16[256,64]{0,1:T(8,128)(2,1)S(1)}, bf16[256,64]{0,1:T(8,128)(2,1)}, u32[]{:S(2)}) copy-start(bf16[256,64]{0,1:T(8,128)(2,1)} %param.27) | copy-start | bytes 98308
  138.3 4.8 %copy-start.7 = (bf16[256,64]{0,1:T(8,128)(2,1)S(1)}, bf16[256,64]{0,1:T(8,128)(2,1)}, u32[]{:S(2)}) copy-start(bf16[256,64]{0,1:T(8,128)(2,1)} %param.26) | copy-start | bytes 98308
  163.9 123.6 %copy-start.2 = (bf16[64,2048]{1,0:T(8,128)(2,1)S(1)}, bf16[64,2048]{1,0:T(8,128)(2,1)}, u32[]{:S(2)}) copy-start(bf16[64,2048]{1,0:T(8,128)(2,1)} %param.28) | copy-start | bytes 786436
  287.5 5.8 %copy-start.3 = (f32[128,2]{0,1:T(2,128)S(1)}, f32[128,2]{0,1:T(2,128)}, u32[]{:S(2)}) copy-start(f32[128,2]{0,1:T(2,128)} %param.32) | copy-start | bytes 3076
  289.6 36.6 %all-to-all-start = ((bf16[16,32,2048]{2,1,0:T(8,128)(2,1)}), bf16[16,32,2048]{2,1,0:T(8,128)(2,1)S(1)}, u32[]{:S(2)}, u32[]{:S(2)}) async-start(bf16[16,32,2048]{2,1,0:T(8,128)(2,1)} %bitcast.9), calls=%async_computation | async-start | bytes 4194304 | tf_op jit(solution)/shard_map/all_to_all | solution.py:31
Sparse Core Ops, SparseCore 0:
  10.1 90.2 all-gather.1
where the time goes:
time: 337 us; the launch traced here: 334 us
  matrix products  139 us (41%)
  blocking collectives  62.9 us (19%)
  waiting for transfers between devices  49.2 us (15%)
  other arithmetic  25.9 us (8%)
  local copies, waits for them, and re-layouts  23.7 us (7%)
  starting transfers between devices  17.4 us (5%)
  between operations  14.4 us (4%)
    all_to_all x2, waiting for transfers between devices, sent_and_summed(): lax.all_to_all(pieces, axis, split_axis=0, concat_axis=0, tiled=True)  49.2 us
    dot_general x32, matrix products, attend_block(): jnp.einsum('hqk,khd->hqd', weights.astype(jnp.bfloat16), value_heads, pre...  39.3 us
    dot_general x32, matrix products, attend_block(): jnp.einsum('qhd,khd->hqk', q_nope, key_heads, preferred_element_type=jnp....  38.2 us
    dot_general x32, matrix products, attend_block(): jnp.einsum('qhr,kr->hqk', q_rope, k_rope, preferred_element_type=jnp.floa...  37.4 us
    all_to_all x1, blocking collectives, shards(): lax.all_to_all(outgoing, 'ep', split_axis=0, concat_axis=0, tiled=True)  34.7 us
    all_to_all x1, blocking collectives, from_everyone(): return lax.all_to_all(copies, axis, split_axis=0, concat_axis=0, tiled=True)  28.2 us
    unnamed x23, local copies, waits for them, and re-layouts  14.8 us
    all_to_all x1, starting transfers between devices, shards(): lax.all_to_all(finished, 'ep', split_axis=0, concat_axis=0, tiled=True)  9.95 us
  transfers between devices with their start and end apart: 4, of which 2 were waited for; matrix products, arithmetic and copies ran while one was open for 55% of the time, Pallas kernels for 0%

commit v1 on v0

v1 whole, which is shorter than its diff:
```python
import math

import jax
import jax.numpy as jnp
from jax import lax
from jax.experimental import pallas as pl
from jax.experimental.pallas import tpu as pltpu
from jax.sharding import Mesh, PartitionSpec as P


NOPE = 64
ROPE = 32
VDIM = 64
EPSILON = 1e-06
EP = ("z", "c")
TP = ("y", "x")
F32 = jnp.float32
BF16 = jnp.bfloat16
MIB = 1 << 20


def params(mib):
    return pltpu.CompilerParams(vmem_limit_bytes=mib * MIB)


def turns(places, half):
    freqs = 10000.0 ** (-jnp.arange(half, dtype=F32) / half)
    angles = freqs[:, None] * places.astype(F32)[None, :]
    return jnp.cos(angles), jnp.sin(angles)


def dispatch_kernel(experts, room, at_ref, tokens_ref, gain_ref, routes_ref, out_ref, where_ref):
    rows, width = tokens_ref.shape
    share, pitch = out_ref.shape[2], 16 * (-(-room // 16))
    wide = tokens_ref[...].astype(F32)
    mean = jnp.sum(wide * wide, axis=-1, keepdims=True) * (1.0 / width)
    start = pl.multiple_of(at_ref[0] * share, share)
    mine = tokens_ref[:, pl.ds(start, share)].astype(F32) * lax.rsqrt(mean + EPSILON)
    normed = (mine * gain_ref[:, pl.ds(start, share)].astype(F32)).astype(BF16)
    names = lax.broadcasted_iota(jnp.int32, (experts, rows), 0)
    first, second = routes_ref[0:1, :], routes_ref[1:2, :]
    hit_first = jnp.where(names == first, 1.0, 0.0)
    hit_second = jnp.where(names == second, 1.0, 0.0)
    before = lax.broadcasted_iota(jnp.int32, (rows, rows), 0) < lax.broadcasted_iota(
        jnp.int32, (rows, rows), 1
    )
    earlier = jnp.where(before, 1.0, 0.0).astype(BF16)
    seen = jnp.dot((hit_first + hit_second).astype(BF16), earlier, preferred_element_type=F32)
    slot_first = jnp.sum(seen * hit_first, axis=0, keepdims=True)
    slot_second = jnp.sum(seen * hit_second, axis=0, keepdims=True)
    to_first = first * pitch + slot_first.astype(jnp.int32)
    to_second = second * pitch + slot_second.astype(jnp.int32)
    where_ref[0:1, :] = to_first
    where_ref[1:2, :] = to_second
    places = lax.broadcasted_iota(jnp.int32, (experts * pitch, rows), 0)
    chosen = jnp.where((places == to_first) | (places == to_second), 1.0, 0.0).astype(BF16)
    picked = jnp.dot(chosen, normed, preferred_element_type=F32).astype(BF16)
    out_ref[...] = picked.reshape(experts, pitch, share)[:, :room]


def dispatch(tokens, gain, routes, at, experts, room, share):
    rows = tokens.shape[0]
    vmem = pl.BlockSpec(memory_space=pltpu.VMEM)
    return pl.pallas_call(
        lambda *refs: dispatch_kernel(experts, room, *refs),
        out_shape=(
            jax.ShapeDtypeStruct((experts, room, share), BF16),
            jax.ShapeDtypeStruct((2, rows), jnp.int32),
        ),
        in_specs=[pl.BlockSpec(memory_space=pltpu.SMEM), vmem, vmem, vmem],
        out_specs=(vmem, vmem),
        compiler_params=params(60),
        cost_estimate=pl.CostEstimate(flops=10_000_000, bytes_accessed=700_000, transcendentals=0),
        name="dispatch",
    )(at, tokens, gain.reshape(1, -1), routes.T)


def expert_kernel(x_ref, gate_hbm, up_hbm, down_hbm, out_ref, gate_ref, up_ref, down_ref, sems):
    pieces, rows, share = x_ref.shape
    loads = [
        pltpu.make_async_copy(source, target, sems.at[n])
        for n, (source, target) in enumerate(
            ((gate_hbm, gate_ref), (up_hbm, up_ref), (down_hbm, down_ref))
        )
    ]
    for load in loads:
        load.start()
    loads[0].wait()
    loads[1].wait()
    step = 128
    for at in range(0, rows, step):
        x = jnp.concatenate([x_ref[p, at : at + step, :] for p in range(pieces)], axis=1)
        gate = jnp.dot(x, gate_ref[...], preferred_element_type=F32)
        up = jnp.dot(x, up_ref[...], preferred_element_type=F32)
        hidden = (gate / (1.0 + jnp.exp(-gate)) * up).astype(BF16)
        if at == 0:
            loads[2].wait()
        for p in range(0, pieces, 2):
            term = jnp.dot(
                hidden, down_ref[:, p * share : (p + 2) * share], preferred_element_type=F32
            ).astype(BF16)
            out_ref[p, at : at + step, :] = term[:, :share]
            out_ref[p + 1, at : at + step, :] = term[:, share:]


def expert(x, gate, up, down):
    vmem = pl.BlockSpec(memory_space=pltpu.VMEM)
    return pl.pallas_call(
        expert_kernel,
        out_shape=jax.ShapeDtypeStruct(x.shape, BF16),
        in_specs=[vmem] + [pl.BlockSpec(memory_space=pl.ANY)] * 3,
        out_specs=vmem,
        scratch_shapes=[pltpu.VMEM(w.shape, BF16) for w in (gate, up, down)]
        + [pltpu.SemaphoreType.DMA((3,))],
        compiler_params=params(56),
        cost_estimate=pl.CostEstimate(flops=40_000_000, bytes_accessed=6_000_000, transcendentals=0),
        name="expert",
    )(x, gate, up, down)


def combine_kernel(back_ref, where_ref, logits_ref, out_ref, wide_ref):
    rows, share = out_ref.shape
    wide_ref[...] = jnp.zeros_like(wide_ref)
    wide_ref[:, : back_ref.shape[1]] = back_ref[...]
    back = wide_ref[...].reshape(-1, share)
    places = lax.broadcasted_iota(jnp.int32, (rows, back.shape[0]), 1)
    left, right = logits_ref[:, 0:1], logits_ref[:, 1:2]
    top = jnp.maximum(left, right)
    grow_left, grow_right = jnp.exp(left - top), jnp.exp(right - top)
    both = grow_left + grow_right
    mixed = jnp.zeros(out_ref.shape, F32)
    for k, grown in ((0, grow_left), (1, grow_right)):
        chosen = jnp.where(places == where_ref[:, k : k + 1], 1.0, 0.0).astype(BF16)
        picked = jnp.dot(chosen, back, preferred_element_type=F32)
        mixed = mixed + picked * (grown / both)
    out_ref[...] = mixed.astype(BF16)


def combine(back, where, logits):
    vmem = pl.BlockSpec(memory_space=pltpu.VMEM)
    return pl.pallas_call(
        combine_kernel,
        out_shape=jax.ShapeDtypeStruct((logits.shape[0], back.shape[2]), BF16),
        in_specs=[vmem] * 3,
        out_specs=vmem,
        scratch_shapes=[pltpu.VMEM((back.shape[0], 16 * (-(-back.shape[1] // 16)), back.shape[2]), BF16)],
        compiler_params=params(8),
        name="combine",
    )(back, where, logits)


def normed_rows(ref, gain_ref):
    wide = ref[...].astype(F32)
    mean = jnp.sum(wide * wide, axis=-1, keepdims=True) * (1.0 / ref.shape[1])
    return (wide * lax.rsqrt(mean + EPSILON) * gain_ref[...].astype(F32)).astype(BF16)


def across(left, right):
    return lax.dot_general(left, right, (((1,), (1,)), ((), ())), preferred_element_type=F32)


def turned(values, cosine, sine):
    half = values.shape[0] // 2
    first, second = values[:half], values[half:]
    return first * cosine - second * sine, first * sine + second * cosine


def keys_kernel(kv_ref, gain_ref, rope_ref, key_ref, value_ref, cos_ref, sin_ref, out_ref):
    normed = normed_rows(kv_ref, gain_ref)
    half = ROPE // 2
    first, second = turned(rope_ref[...].astype(F32), cos_ref[...], sin_ref[...])
    out_ref[:NOPE] = across(key_ref[...], normed).astype(BF16)
    out_ref[NOPE : NOPE + half] = first.astype(BF16)
    out_ref[NOPE + half : NOPE + ROPE] = second.astype(BF16)
    out_ref[NOPE + ROPE :] = across(value_ref[...], normed).astype(BF16)


def keys(kv, gain, rope_key, w_key, w_value, cosine, sine):
    vmem = pl.BlockSpec(memory_space=pltpu.VMEM)
    return pl.pallas_call(
        keys_kernel,
        out_shape=jax.ShapeDtypeStruct((NOPE + ROPE + VDIM, kv.shape[0]), BF16),
        in_specs=[vmem] * 7,
        out_specs=vmem,
        compiler_params=params(60),
        cost_estimate=pl.CostEstimate(flops=10_000_000, bytes_accessed=500_000, transcendentals=0),
        name="keys",
    )(kv, gain.reshape(1, -1), rope_key.T, w_key.T, w_value.T, cosine, sine)


def queries_kernel(side, q_ref, gain_ref, nope_ref, rope_ref, cos_ref, sin_ref, out_ref):
    normed = normed_rows(q_ref, gain_ref)
    rows = normed.shape[0]
    few = rows // (side * side)
    order = [(y * side + x) * few for x in range(side) for y in range(side)]
    normed = jnp.concatenate([normed[at : at + few] for at in order], axis=0)
    half = ROPE // 2
    out_ref[:NOPE] = across(nope_ref[...], normed).astype(BF16)
    first, second = turned(across(rope_ref[...], normed), cos_ref[...], sin_ref[...])
    out_ref[NOPE : NOPE + half] = first.astype(BF16)
    out_ref[NOPE + half : NOPE + ROPE] = second.astype(BF16)
    out_ref[NOPE + ROPE :] = jnp.zeros((out_ref.shape[0] - NOPE - ROPE, rows), BF16)


def queries(q_latent, gain, w_nope, w_rope, cosine, sine, side):
    vmem = pl.BlockSpec(memory_space=pltpu.VMEM)
    return pl.pallas_call(
        lambda *refs: queries_kernel(side, *refs),
        out_shape=jax.ShapeDtypeStruct((128, q_latent.shape[0]), BF16),
        in_specs=[vmem] * 6,
        out_specs=vmem,
        compiler_params=params(60),
        cost_estimate=pl.CostEstimate(flops=10_000_000, bytes_accessed=700_000, transcendentals=0),
        name="queries",
    )(q_latent, gain.reshape(1, -1), w_nope.T, w_rope.T, cosine, sine)


def attention_kernel(q_ref, own_ref, other_ref, out_ref, s_ref, acc_ref):
    tile = 256
    blocks, _, span = own_ref.shape
    queries = q_ref.shape[1]
    cut = NOPE + ROPE
    rate = (NOPE + ROPE) ** (-0.5) * math.log2(math.e)
    pad = jnp.zeros((q_ref.shape[0] - cut, tile), BF16)
    ones = jnp.ones((16, tile), BF16)
    tiles = [(ref, at) for ref in (own_ref, other_ref) for at in range(0, span, tile)]
    halves = range(0, queries, tile)

    def score(block, slot, top):
        tops = [None for _ in halves]
        for n, (ref, at) in enumerate(tiles):
            keys = jnp.concatenate([ref[block, :cut, at : at + tile], pad], axis=0).T
            for i, h in enumerate(halves):
                s = jnp.dot(keys, q_ref[:, h : h + tile], preferred_element_type=F32)
                s_ref[slot, n * tile : (n + 1) * tile, h : h + tile] = s
                most = jnp.max(s.reshape(tile // 8, 8, tile), axis=0)
                tops[i] = most if tops[i] is None else jnp.maximum(tops[i], most)
        block_top = jnp.max(jnp.concatenate(tops, axis=1), axis=0, keepdims=True)
        return jnp.maximum(top, block_top)

    def absorb(block, slot, old_top, top):
        shrink = jnp.exp2((old_top - top) * rate)
        for h in halves:
            total = acc_ref[:, h : h + tile] * shrink[:, h : h + tile]
            for n, (ref, at) in enumerate(tiles):
                s = s_ref[slot, n * tile : (n + 1) * tile, h : h + tile]
                weights = jnp.exp2((s - top[:, h : h + tile]) * rate).astype(BF16)
                rows = jnp.concatenate([ref[block, cut:, at : at + tile], ones], axis=0)
                total = total + jnp.dot(rows, weights, preferred_element_type=F32)
            acc_ref[:, h : h + tile] = total

    def pair(turn, carry):
        old_top, top = carry
        for slot in (0, 1):
            block = turn * 2 + slot
            ahead = jnp.minimum(block + 1, blocks - 1)
            new_top = score(ahead, 1 - slot, top)
            absorb(block, slot, old_top, top)
            old_top, top = top, new_top
        return old_top, top

    acc_ref[...] = jnp.zeros_like(acc_ref)
    floor = jnp.full((1, queries), -1e30, F32)
    lax.fori_loop(0, blocks // 2, pair, (floor, score(0, 0, floor)))

    done = (acc_ref[:VDIM, :] / acc_ref[VDIM : VDIM + 1, :]).astype(BF16)
    for n in range(out_ref.shape[0]):
        out_ref[n] = done[:, n * out_ref.shape[2] : (n + 1) * out_ref.shape[2]]


def attention(q, own, other, parts):
    vmem = pl.BlockSpec(memory_space=pltpu.VMEM)
    queries = q.shape[1]
    return pl.pallas_call(
        attention_kernel,
        out_shape=jax.ShapeDtypeStruct((parts, VDIM, queries // parts), BF16),
        in_specs=[vmem] * 3,
        out_specs=vmem,
        scratch_shapes=[
            pltpu.VMEM((2, 2 * own.shape[2], queries), F32),
            pltpu.VMEM((VDIM + 16, queries), F32),
        ],
        compiler_params=params(24),
        cost_estimate=pl.CostEstimate(flops=200_000_000, bytes_accessed=8_000_000, transcendentals=0),
        name="attention",
    )(q, own, other)


def ring(count, step):
    return [(i, (i + step) % count) for i in range(count)]


def from_row(value, axis):
    count = lax.axis_size(axis)
    return [value] + [lax.ppermute(value, axis, ring(count, k)) for k in range(1, count)]


def traded(pieces, axis):
    count, me = lax.axis_size(axis), lax.axis_index(axis)
    mine = lambda k: lax.dynamic_index_in_dim(pieces, lax.rem(me + k, count), 0, False, allow_negative_indices=False)
    return [mine(0)] + [
        lax.ppermute(mine(k), axis, ring(count, k)) for k in range(1, count)
    ]


def shards(
    q_latent,
    kv_latent,
    rope_key,
    q_gain,
    kv_gain,
    w_q_nope,
    w_q_rope,
    w_k_nope,
    w_value,
    w_out,
    tokens_b,
    norm_gain_b,
    routes,
    route_logits,
    w_gate,
    w_up,
    w_down,
):
    n_ep, n_tp = lax.axis_size(EP), lax.axis_size(TP)
    side = lax.axis_size("x")
    rows_b, width = tokens_b.shape
    room = 3 * rows_b // n_ep
    share = width // n_tp
    own_rows = q_latent.shape[0]
    first_row = lax.axis_index(EP) * own_rows
    places = jnp.arange(own_rows, dtype=jnp.int32)
    cos_k, sin_k = turns(first_row + places, ROPE // 2)
    mixed = places.reshape(side, side, -1).transpose(1, 0, 2).reshape(-1)
    cos_q, sin_q = turns(first_row + mixed, ROPE // 2)
    piece = keys(kv_latent, kv_gain, rope_key, w_k_nope, w_value, cos_k, sin_k)
    own = lax.all_gather(piece, "z", axis=0, tiled=False)
    routes, piece = lax.optimization_barrier((routes, piece))
    outgoing, where = dispatch(
        tokens_b, norm_gain_b, routes, lax.axis_index(TP)[None], n_ep, room, share
    )
    arrived = lax.all_to_all(outgoing, EP, split_axis=0, concat_axis=0, tiled=True)
    w_group = jnp.concatenate(from_row(w_out, "x"), axis=0)
    q = queries(q_latent, q_gain, w_q_nope, w_q_rope, cos_q, sin_q, side)
    mine = arrived.reshape(1, n_ep * room, share)
    mine = jnp.broadcast_to(mine, (n_tp, n_ep * room, share))
    rows = lax.all_to_all(mine, TP, split_axis=0, concat_axis=0, tiled=True)
    terms = expert(rows, w_gate[0], w_up[0], w_down[0])
    terms = lax.all_to_all(terms, TP, split_axis=0, concat_axis=0, tiled=True)
    other = lax.ppermute(own, "c", [(0, 1), (1, 0)])
    heads = attention(q, own, other, side)
    heads = jnp.concatenate(traded(heads, "x"), axis=0)
    partial = lax.dot_general(
        heads, w_group, (((0,), (0,)), ((), ())), preferred_element_type=F32
    ).astype(BF16)
    partial = partial.reshape(side, own_rows // n_tp, width)
    partial = traded(partial, "y")
    finished = terms.astype(F32).sum(axis=0).astype(BF16)
    back = lax.all_to_all(
        finished.reshape(n_ep, room, share), EP, split_axis=0, concat_axis=0, tiled=True
    )
    expert_mix = combine(back, where.T, route_logits)
    mixer_out = sum(p.astype(F32) for p in partial).astype(BF16)
    return (mixer_out, expert_mix)


def solution(mesh):
    n_ep, n_tp = mesh.shape["ep"], mesh.shape["tp"]
    side = math.isqrt(n_tp)
    split = Mesh(
        mesh.devices.reshape(n_ep // 2, 2, side, n_tp // side), ("z", "c", "y", "x")
    )
    placed = (
        P(EP, None),
        P(EP, None),
        P(EP, None),
        P(),
        P(),
        P(None, TP),
        P(None, TP),
        P(None, TP),
        P(None, TP),
        P(TP, None),
        P(EP, None),
        P(),
        P(EP, None),
        P(EP, None),
        P(EP, None, TP),
        P(EP, None, TP),
        P(EP, TP, None),
    )
    return jax.shard_map(
        shards,
        mesh=split,
        in_specs=placed,
        out_specs=(P(EP + TP, None), P(EP, TP)),
        check_vma=False,
    )
```

time: 337 us -> 182 us (0.54)
  matrix products: 139 us -> 1.29 us
  starting transfers between devices: 17.4 us -> 62.7 us
  blocking collectives: 62.9 us -> 33.4 us
  Pallas kernels: 0 us -> 25.3 us
  other arithmetic: 25.9 us -> 3.32 us
  waiting for transfers between devices: 49.2 us -> 33 us
  local copies, waits for them, and re-layouts: 23.7 us -> 7.82 us
    dot_general x103 -> x1, matrix products: 139 us -> 1.29 us  [shards(): lax.dot_general(heads, w_group, (((0,), (0,)), ((), ())), preferred_eleme...]
    all_to_all x3, waiting for transfers between devices: 49.2 us -> 3.68 us  [the longest x1 3.68 us: shards(): lax.all_to_all(finished.reshape(n_ep, room, share), EP, split_axis=0, con...]
    ppermute x0 -> x10, starting transfers between devices: none -> 39.7 us  [the longest x6 18.9 us: traded(): lax.ppermute(mine(k), axis, ring(count, k))]
    all_to_all x2 -> x1, blocking collectives: 62.9 us -> 33.4 us  [shards(): lax.all_to_all(outgoing, EP, split_axis=0, concat_axis=0, tiled=True)]
    all_gather x1, waiting for transfers between devices: 0.02 us -> 29.2 us  [shards(): own = lax.all_gather(piece, 'z', axis=0, tiled=False)]
    pallas_call x0 -> x6, Pallas kernels: none -> 25.3 us  [the longest x1 11.8 us: attention(): pl.pallas_call(attention_kernel, out_shape=jax.ShapeDtypeStruct((parts, V...]
    reduce_sum x40 -> x1, other arithmetic: 15.1 us -> 1.63 us  [shards(): finished = terms.astype(F32).sum(axis=0).astype(BF16)]
    unnamed x23 -> x15, local copies, waits for them, and re-layouts: 14.8 us -> 2.27 us
  transfers between devices with their start and end apart: 4 -> 14, of which waited for: 2 -> 2; matrix products, arithmetic and copies ran while one was open for 55% -> 4% of each run, Pallas kernels for 0% -> 13%
where the time goes in v1:
time: 182 us; the launch traced here: 181 us
  starting transfers between devices  62.7 us (34%)
  blocking collectives  33.4 us (18%)
  waiting for transfers between devices  33 us (18%)
  Pallas kernels  25.3 us (14%)
  between operations  14.4 us (8%)
  local copies, waits for them, and re-layouts  7.82 us (4%)
  other arithmetic  3.32 us (2%)
    all_to_all x1, blocking collectives, shards(): lax.all_to_all(outgoing, EP, split_axis=0, concat_axis=0, tiled=True)  33.4 us
    all_gather x1, waiting for transfers between devices, shards(): own = lax.all_gather(piece, 'z', axis=0, tiled=False)  29.2 us
    ppermute x6, starting transfers between devices, traded(): lax.ppermute(mine(k), axis, ring(count, k))  18.9 us
    pallas_call x1, Pallas kernels, attention(): pl.pallas_call(attention_kernel, out_shape=jax.ShapeDtypeStruct((parts, V...  11.8 us
    ppermute x3, starting transfers between devices, from_row(): lax.ppermute(value, axis, ring(count, k))  10.6 us
    ppermute x1, starting transfers between devices, shards(): other = lax.ppermute(own, 'c', [(0, 1), (1, 0)])  10.1 us
    all_to_all x1, starting transfers between devices, shards(): lax.all_to_all(finished.reshape(n_ep, room, share), EP, split_axis=0, con...  9.11 us
    all_to_all x1, starting transfers between devices, shards(): terms = lax.all_to_all(terms, TP, split_axis=0, concat_axis=0, tiled=True)  7.01 us
  transfers between devices with their start and end apart: 14, of which 2 were waited for; matrix products, arithmetic and copies ran while one was open for 4% of the time, Pallas kernels for 13%

profile of v1, /device:TPU:1, one launch (start us, length us, event | category | flops | bytes accessed | tf_op | source)
XLA Modules:
  0.0 181.2 jit_solution(15572160899487029197)
XLA Ops:
  7.3 1.2 reshape.84.gain_ref
  8.6 0.9 multiply_sine_fusion
  9.5 2.0 %keys.1 = bf16[160,512]{1,0:T(8,128)(2,1)} custom-call(bf16[512,256]{1,0:T(8,128)(2,1)} %kv_ref.1, bf16[1,256]{1,0:T(2,128)(2,1)} %reshape.84.gain_ref, bf16[32,512]{1,0:T(8,128)(2,1)} %bitcast.39, bf16[64,256]{1,0:T(8,128)(2,1)} %bitcast.40, bf16[64,256]{1,0:T(8,128)(2,1)} %bitcast.41, f32[16,512]{1,0:T(8,128)} %get-tuple-element.16.cos_ref, ...), custom_call_target="tpu_custom_call" | custom-call | flops 10000000 | bytes 500000 | tf_op jit(solution)/shard_map/keys/pallas_call | solution.py:180
  11.6 1.3 reshape.86.refs_2_
  12.9 2.1 %dispatch.1 = (bf16[32,12,128]{2,1,0:T(8,128)(2,1)}, s32[2,128]{1,0:T(2,128)}) custom-call(s32[1]{0:T(128)} %bitcast.15.refs_0_, bf16[128,2048]{1,0:T(8,128)(2,1)} %refs_1_.1, bf16[1,2048]{1,0:T(2,128)(2,1)} %reshape.86.refs_2_, s32[2,128]{1,0:T(2,128)} %bitcast.43), custom_call_target="tpu_custom_call" | custom-call | flops 10000000 | bytes 700000 | tf_op jit(solution)/shard_map/dispatch/pallas_call | solution.py:64
  15.0 33.4 %all_to_all.20 = bf16[32,12,128]{2,1,0:T(8,128)(2,1)S(1)} all-to-all(bf16[32,12,128]{2,1,0:T(8,128)(2,1)} %get-tuple-element.6), channel_id=1, replica_groups=mesh['z'=16,'c'=2,'y'=4,'x'=4] {'z','c'}, dimensions={0} | all-to-all | bytes 196608 | tf_op jit(solution)/shard_map/all_to_all | solution.py:342
  48.4 1.5 broadcast_in_dim.16
  49.9 6.9 %all-to-all-start.1 = ((bf16[16,384,128]{2,1,0:T(8,128)(2,1)}), bf16[16,384,128]{2,1,0:T(8,128)(2,1)S(1)}, u32[]{:S(2)}, u32[]{:S(2)}) async-start(bf16[16,384,128]{2,1,0:T(8,128)(2,1)} %broadcast_in_dim.16), calls=%async_computation.1 | async-start | bytes 3145728 | tf_op jit(solution)/shard_map/all_to_all | solution.py:347
  56.8 29.2 %all-gather.3.cloned.1.call-done = bf16[2560,512]{1,0:T(8,128)(2,1)} async-done(((bf16[160,512]{1,0:T(8,128)(2,1)}), bf16[2560,512]{1,0:T(8,128)(2,1)}) %all-gather.3.cloned.1.call-update) | async-done | bytes 2621456 | tf_op jit(solution)/shard_map/all_gather | solution.py:337
  86.0 10.1 %collective-permute-start = (bf16[16,160,512]{2,1,0:T(8,128)(2,1)}, bf16[16,160,512]{2,1,0:T(8,128)(2,1)}, u32[]{:S(2)}, u32[]{:S(2)}) collective-permute-start(bf16[16,160,512]{2,1,0:T(8,128)(2,1)} %bitcast.30), channel_id=1, source_target_pairs={{0,16},{16,0},{1,17},{17,1},{2,18},{18,2},{3,19},{19,3},{4,20},{20... | collective-permute-start | bytes 7864328 | tf_op jit(solution)/shard_map/ppermute | solution.py:350
  96.2 1.2 copy-done.2
  97.4 6.0 %expert.1 = bf16[16,384,128]{2,1,0:T(8,128)(2,1)} custom-call(bf16[16,384,128]{2,1,0:T(8,128)(2,1)} %copy-done.2, bf16[2048,256]{1,0:T(8,128)(2,1)} %bitcast.33, bf16[2048,256]{1,0:T(8,128)(2,1)} %bitcast.34, bf16[256,2048]{1,0:T(8,128)(2,1)} %bitcast.35), custom_call_target="tpu_custom_call" | custom-call | flops 40000000 | bytes 6000000 | tf_op jit(solution)/shard_map/expert/pallas_call | solution.py:108
  103.5 7.0 %all-to-all-start.2 = ((bf16[16,384,128]{2,1,0:T(8,128)(2,1)}), bf16[16,384,128]{2,1,0:T(8,128)(2,1)}, u32[]{:S(2)}, u32[]{:S(2)}) async-start(bf16[16,384,128]{2,1,0:T(8,128)(2,1)} %expert.1), calls=%async_computation.2 | async-start | bytes 3145728 | tf_op jit(solution)/shard_map/all_to_all | solution.py:349
  110.5 3.2 %collective-permute-start.4 = (bf16[64,2048]{1,0:T(8,128)(2,1)S(1)}, bf16[64,2048]{1,0:T(8,128)(2,1)S(1)}, u32[]{:S(2)}, u32[]{:S(2)}) collective-permute-start(bf16[64,2048]{1,0:T(8,128)(2,1)S(1)} %copy-done.6), channel_id=1, source_target_pairs={{0,1},{1,2},{2,3},{3,0},{4,5},{5,6},{6,7},{7,4},{8,9},{9,10},{10,1... | collective-permute-start | bytes 786440 | tf_op jit(solution)/shard_map/ppermute | solution.py:295
  113.7 4.3 %collective-permute-start.5 = (bf16[64,2048]{1,0:T(8,128)(2,1)S(1)}, bf16[64,2048]{1,0:T(8,128)(2,1)S(1)}, u32[]{:S(2)}, u32[]{:S(2)}) collective-permute-start(bf16[64,2048]{1,0:T(8,128)(2,1)S(1)} %copy-done.6), channel_id=1, source_target_pairs={{0,2},{1,3},{2,0},{3,1},{4,6},{5,7},{6,4},{7,5},{8,10},{9,11},{10,... | collective-permute-start | bytes 786440 | tf_op jit(solution)/shard_map/ppermute | solution.py:295
  118.1 3.1 %collective-permute-start.6 = (bf16[64,2048]{1,0:T(8,128)(2,1)S(1)}, bf16[64,2048]{1,0:T(8,128)(2,1)}, u32[]{:S(2)}, u32[]{:S(2)}) collective-permute-start(bf16[64,2048]{1,0:T(8,128)(2,1)S(1)} %copy-done.6), channel_id=1, source_target_pairs={{0,3},{1,0},{2,1},{3,2},{4,7},{5,4},{6,5},{7,6},{8,11},{9,8},{10,9... | collective-permute-start | bytes 786440 | tf_op jit(solution)/shard_map/ppermute | solution.py:295
  121.7 2.3 %queries.1.q_ref = bf16[128,512]{1,0:T(8,128)(2,1)} custom-call(bf16[512,512]{1,0:T(8,128)(2,1)} %refs_0_.1, bf16[1,512]{1,0:T(2,128)(2,1)} %reshape.77.refs_1_, bf16[64,512]{1,0:T(8,128)(2,1)} %bitcast.38, bf16[32,512]{1,0:T(8,128)(2,1)} %bitcast.42, f32[16,512]{1,0:T(8,128)} %get-tuple-element.19.refs_4_, f32[16,512]{1,0:T(8,128)} %get-tuple-element.20.refs_5_), custom_call_target="tpu_custom_call" | custom-call | flops 10000000 | bytes 700000 | tf_op jit(solution)/shard_map/queries/pallas_call | solution.py:207
  124.0 0.9 copy-done.1
  124.9 11.8 %attention.1 = bf16[4,64,128]{2,1,0:T(8,128)(2,1)S(1)} custom-call(bf16[128,512]{1,0:T(8,128)(2,1)S(1)} %copy-done.1, bf16[16,160,512]{2,1,0:T(8,128)(2,1)S(1)} %bitcast.31, bf16[16,160,512]{2,1,0:T(8,128)(2,1)} %collective-permute-done.other_ref), custom_call_target="tpu_custom_call" | custom-call | flops 200000000 | bytes 8000000 | tf_op jit(solution)/shard_map/attention/pallas_call | solution.py:274
  136.8 2.2 %collective-permute-start.1 = (bf16[64,128]{1,0:T(8,128)(2,1)S(1)}, bf16[64,128]{1,0:T(8,128)(2,1)S(1)}, u32[]{:S(2)}, u32[]{:S(2)}) collective-permute-start(bf16[64,128]{1,0:T(8,128)(2,1)S(1)} %get-tuple-element.14), channel_id=1, source_target_pairs={{0,1},{1,2},{2,3},{3,0},{4,5},{5,6},{6,7},{7,4},{8,9},{9,10},{10,1... | collective-permute-start | bytes 49160 | tf_op jit(solution)/shard_map/ppermute | solution.py:302
  139.0 2.8 %collective-permute-start.2 = (bf16[64,128]{1,0:T(8,128)(2,1)S(1)}, bf16[64,128]{1,0:T(8,128)(2,1)S(1)}, u32[]{:S(2)}, u32[]{:S(2)}) collective-permute-start(bf16[64,128]{1,0:T(8,128)(2,1)S(1)} %get-tuple-element.13), channel_id=1, source_target_pairs={{0,2},{1,3},{2,0},{3,1},{4,6},{5,7},{6,4},{7,5},{8,10},{9,11},{10,... | collective-permute-start | bytes 49160 | tf_op jit(solution)/shard_map/ppermute | solution.py:302
  141.9 3.4 %collective-permute-start.3 = (bf16[64,128]{1,0:T(8,128)(2,1)S(1)}, bf16[64,128]{1,0:T(8,128)(2,1)S(1)}, u32[]{:S(2)}, u32[]{:S(2)}) collective-permute-start(bf16[64,128]{1,0:T(8,128)(2,1)S(1)} %get-tuple-element.12), channel_id=1, source_target_pairs={{0,3},{1,0},{2,1},{3,2},{4,7},{5,4},{6,5},{7,6},{8,11},{9,8},{10,9... | collective-permute-start | bytes 49160 | tf_op jit(solution)/shard_map/ppermute | solution.py:302
  145.3 1.6 reduce_sum.12
  146.9 0.7 reshape.87
  147.6 9.1 %all-to-all-start.3 = ((bf16[32,12,128]{2,1,0:T(8,128)(2,1)}), bf16[32,12,128]{2,1,0:T(8,128)(2,1)S(1)}, u32[]{:S(2)}, u32[]{:S(2)}) async-start(bf16[32,12,128]{2,1,0:T(8,128)(2,1)} %reshape.87), calls=%async_computation.3 | async-start | bytes 262144 | tf_op jit(solution)/shard_map/all_to_all | solution.py:359
  156.8 1.3 convolution_convert_fusion
  158.1 3.1 %collective-permute-start.7 = (bf16[32,2048]{1,0:T(8,128)(2,1)S(1)}, bf16[32,2048]{1,0:T(8,128)(2,1)S(1)}, u32[]{:S(2)}, u32[]{:S(2)}) collective-permute-start(bf16[32,2048]{1,0:T(8,128)(2,1)S(1)} %get-tuple-element.8), channel_id=1, source_target_pairs={{0,4},{4,8},{8,12},{12,0},{1,5},{5,9},{9,13},{13,1},{2,6},{6,10},{... | collective-permute-start | bytes 393224 | tf_op jit(solution)/shard_map/ppermute | solution.py:302
  161.3 4.3 %collective-permute-start.8 = (bf16[32,2048]{1,0:T(8,128)(2,1)S(1)}, bf16[32,2048]{1,0:T(8,128)(2,1)S(1)}, u32[]{:S(2)}, u32[]{:S(2)}) collective-permute-start(bf16[32,2048]{1,0:T(8,128)(2,1)S(1)} %get-tuple-element.10), channel_id=1, source_target_pairs={{0,8},{4,12},{8,0},{12,4},{1,9},{5,13},{9,1},{13,5},{2,10},{6,14},... | collective-permute-start | bytes 393224 | tf_op jit(solution)/shard_map/ppermute | solution.py:302
  165.6 3.1 %collective-permute-start.9 = (bf16[32,2048]{1,0:T(8,128)(2,1)S(1)}, bf16[32,2048]{1,0:T(8,128)(2,1)S(1)}, u32[]{:S(2)}, u32[]{:S(2)}) collective-permute-start(bf16[32,2048]{1,0:T(8,128)(2,1)S(1)} %get-tuple-element.9), channel_id=1, source_target_pairs={{0,12},{4,0},{8,4},{12,8},{1,13},{5,1},{9,5},{13,9},{2,14},{6,2},{... | collective-permute-start | bytes 393224 | tf_op jit(solution)/shard_map/ppermute | solution.py:302
  168.9 3.7 %all-to-all-done.3.back_ref = bf16[32,12,128]{2,1,0:T(8,128)(2,1)S(1)} async-done(((bf16[32,12,128]{2,1,0:T(8,128)(2,1)}), bf16[32,12,128]{2,1,0:T(8,128)(2,1)S(1)}, u32[]{:S(2)}, u32[]{:S(2)}) %all-to-all-start.3) | async-done | bytes 98336 | tf_op jit(solution)/shard_map/all_to_all | solution.py:359
  172.6 1.0 combine.1
  173.6 0.7 fusion.9
  (36 shorter events, 1.1 us)
Async XLA Ops:
  7.2 78.9 %all-gather.3.cloned.1.call-start = ((), (), s32[]{:S(2)}) async-start(), calls=%async_computation.4 | async-start | bytes 2785280 | tf_op jit(solution)/shard_map/all_gather | solution.py:337
  49.9 46.3 %all-to-all-start.1 = ((bf16[16,384,128]{2,1,0:T(8,128)(2,1)}), bf16[16,384,128]{2,1,0:T(8,128)(2,1)S(1)}, u32[]{:S(2)}, u32[]{:S(2)}) async-start(bf16[16,384,128]{2,1,0:T(8,128)(2,1)} %broadcast_in_dim.16), calls=%async_computation.1 | async-start | bytes 3145728 | tf_op jit(solution)/shard_map/all_to_all | solution.py:347
  86.0 38.0 %collective-permute-start = (bf16[16,160,512]{2,1,0:T(8,128)(2,1)}, bf16[16,160,512]{2,1,0:T(8,128)(2,1)}, u32[]{:S(2)}, u32[]{:S(2)}) collective-permute-start(bf16[16,160,512]{2,1,0:T(8,128)(2,1)} %bitcast.30), channel_id=1, source_target_pairs={{0,16},{16,0},{1,17},{17,1},{2,18},{18,2},{3,19},{19,3},{4,20},{20... | collective-permute-start | bytes 7864328 | tf_op jit(solution)/shard_map/ppermute | solution.py:350
  96.2 1.2 copy-start.2
  103.4 7.1 %copy-start.6 = (bf16[64,2048]{1,0:T(8,128)(2,1)S(1)}, bf16[64,2048]{1,0:T(8,128)(2,1)}, u32[]{:S(2)}) copy-start(bf16[64,2048]{1,0:T(8,128)(2,1)} %param.26) | copy-start | bytes 786436
  103.5 17.7 %copy-start.5 = (bf16[512]{0:T(512)(128)(2,1)S(1)}, bf16[512]{0:T(512)(128)(2,1)}, u32[]{:S(2)}) copy-start(bf16[512]{0:T(512)(128)(2,1)} %param.20) | copy-start | bytes 3076
  103.5 20.6 %copy-start = (bf16[2560,512]{1,0:T(8,128)(2,1)S(1)}, bf16[2560,512]{1,0:T(8,128)(2,1)}, u32[]{:S(2)}) copy-start(bf16[2560,512]{1,0:T(8,128)(2,1)} %all-gather.3.cloned.1.call-done) | copy-start | bytes 7864324
  103.5 41.8 %all-to-all-start.2 = ((bf16[16,384,128]{2,1,0:T(8,128)(2,1)}), bf16[16,384,128]{2,1,0:T(8,128)(2,1)}, u32[]{:S(2)}, u32[]{:S(2)}) async-start(bf16[16,384,128]{2,1,0:T(8,128)(2,1)} %expert.1), calls=%async_computation.2 | async-start | bytes 3145728 | tf_op jit(solution)/shard_map/all_to_all | solution.py:349
  110.5 31.3 %collective-permute-start.4 = (bf16[64,2048]{1,0:T(8,128)(2,1)S(1)}, bf16[64,2048]{1,0:T(8,128)(2,1)S(1)}, u32[]{:S(2)}, u32[]{:S(2)}) collective-permute-start(bf16[64,2048]{1,0:T(8,128)(2,1)S(1)} %copy-done.6), channel_id=1, source_target_pairs={{0,1},{1,2},{2,3},{3,0},{4,5},{5,6},{6,7},{7,4},{8,9},{9,10},{10,1... | collective-permute-start | bytes 786440 | tf_op jit(solution)/shard_map/ppermute | solution.py:295
  113.7 43.0 %collective-permute-start.5 = (bf16[64,2048]{1,0:T(8,128)(2,1)S(1)}, bf16[64,2048]{1,0:T(8,128)(2,1)S(1)}, u32[]{:S(2)}, u32[]{:S(2)}) collective-permute-start(bf16[64,2048]{1,0:T(8,128)(2,1)S(1)} %copy-done.6), channel_id=1, source_target_pairs={{0,2},{1,3},{2,0},{3,1},{4,6},{5,7},{6,4},{7,5},{8,10},{9,11},{10,... | collective-permute-start | bytes 786440 | tf_op jit(solution)/shard_map/ppermute | solution.py:295
  118.1 38.7 %collective-permute-start.6 = (bf16[64,2048]{1,0:T(8,128)(2,1)S(1)}, bf16[64,2048]{1,0:T(8,128)(2,1)}, u32[]{:S(2)}, u32[]{:S(2)}) collective-permute-start(bf16[64,2048]{1,0:T(8,128)(2,1)S(1)} %copy-done.6), channel_id=1, source_target_pairs={{0,3},{1,0},{2,1},{3,2},{4,7},{5,4},{6,5},{7,6},{8,11},{9,8},{10,9... | collective-permute-start | bytes 786440 | tf_op jit(solution)/shard_map/ppermute | solution.py:295
  124.0 0.9 copy-start.1
  136.8 19.9 %collective-permute-start.1 = (bf16[64,128]{1,0:T(8,128)(2,1)S(1)}, bf16[64,128]{1,0:T(8,128)(2,1)S(1)}, u32[]{:S(2)}, u32[]{:S(2)}) collective-permute-start(bf16[64,128]{1,0:T(8,128)(2,1)S(1)} %get-tuple-element.14), channel_id=1, source_target_pairs={{0,1},{1,2},{2,3},{3,0},{4,5},{5,6},{6,7},{7,4},{8,9},{9,10},{10,1... | collective-permute-start | bytes 49160 | tf_op jit(solution)/shard_map/ppermute | solution.py:302
  139.0 17.7 %collective-permute-start.2 = (bf16[64,128]{1,0:T(8,128)(2,1)S(1)}, bf16[64,128]{1,0:T(8,128)(2,1)S(1)}, u32[]{:S(2)}, u32[]{:S(2)}) collective-permute-start(bf16[64,128]{1,0:T(8,128)(2,1)S(1)} %get-tuple-element.13), channel_id=1, source_target_pairs={{0,2},{1,3},{2,0},{3,1},{4,6},{5,7},{6,4},{7,5},{8,10},{9,11},{10,... | collective-permute-start | bytes 49160 | tf_op jit(solution)/shard_map/ppermute | solution.py:302
  141.9 14.9 %collective-permute-start.3 = (bf16[64,128]{1,0:T(8,128)(2,1)S(1)}, bf16[64,128]{1,0:T(8,128)(2,1)S(1)}, u32[]{:S(2)}, u32[]{:S(2)}) collective-permute-start(bf16[64,128]{1,0:T(8,128)(2,1)S(1)} %get-tuple-element.12), channel_id=1, source_target_pairs={{0,3},{1,0},{2,1},{3,2},{4,7},{5,4},{6,5},{7,6},{8,11},{9,8},{10,9... | collective-permute-start | bytes 49160 | tf_op jit(solution)/shard_map/ppermute | solution.py:302
  147.6 25.0 %all-to-all-start.3 = ((bf16[32,12,128]{2,1,0:T(8,128)(2,1)}), bf16[32,12,128]{2,1,0:T(8,128)(2,1)S(1)}, u32[]{:S(2)}, u32[]{:S(2)}) async-start(bf16[32,12,128]{2,1,0:T(8,128)(2,1)} %reshape.87), calls=%async_computation.3 | async-start | bytes 262144 | tf_op jit(solution)/shard_map/all_to_all | solution.py:359
  156.8 11.9 %copy-start.4 = (s32[2,128]{1,0:T(2,128)S(1)}, s32[2,128]{1,0:T(2,128)}, u32[]{:S(2)}) copy-start(s32[2,128]{1,0:T(2,128)} %get-tuple-element.7) | copy-start | bytes 3076
  156.8 12.0 %copy-start.3 = (f32[128,2]{0,1:T(2,128)S(1)}, f32[128,2]{0,1:T(2,128)}, u32[]{:S(2)}) copy-start(f32[128,2]{0,1:T(2,128)} %param.30) | copy-start | bytes 3076
  158.1 15.5 %collective-permute-start.7 = (bf16[32,2048]{1,0:T(8,128)(2,1)S(1)}, bf16[32,2048]{1,0:T(8,128)(2,1)S(1)}, u32[]{:S(2)}, u32[]{:S(2)}) collective-permute-start(bf16[32,2048]{1,0:T(8,128)(2,1)S(1)} %get-tuple-element.8), channel_id=1, source_target_pairs={{0,4},{4,8},{8,12},{12,0},{1,5},{5,9},{9,13},{13,1},{2,6},{6,10},{... | collective-permute-start | bytes 393224 | tf_op jit(solution)/shard_map/ppermute | solution.py:302
  161.3 12.4 %collective-permute-start.8 = (bf16[32,2048]{1,0:T(8,128)(2,1)S(1)}, bf16[32,2048]{1,0:T(8,128)(2,1)S(1)}, u32[]{:S(2)}, u32[]{:S(2)}) collective-permute-start(bf16[32,2048]{1,0:T(8,128)(2,1)S(1)} %get-tuple-element.10), channel_id=1, source_target_pairs={{0,8},{4,12},{8,0},{12,4},{1,9},{5,13},{9,1},{13,5},{2,10},{6,14},... | collective-permute-start | bytes 393224 | tf_op jit(solution)/shard_map/ppermute | solution.py:302
  165.6 8.1 %collective-permute-start.9 = (bf16[32,2048]{1,0:T(8,128)(2,1)S(1)}, bf16[32,2048]{1,0:T(8,128)(2,1)S(1)}, u32[]{:S(2)}, u32[]{:S(2)}) collective-permute-start(bf16[32,2048]{1,0:T(8,128)(2,1)S(1)} %get-tuple-element.9), channel_id=1, source_target_pairs={{0,12},{4,0},{8,4},{12,8},{1,13},{5,1},{9,5},{13,9},{2,14},{6,2},{... | collective-permute-start | bytes 393224 | tf_op jit(solution)/shard_map/ppermute | solution.py:302
Sparse Core Ops, SparseCore 0:
  11.7 74.2 all-gather.2

commit v2 on v1

--- a/solution.py
+++ b/solution.py
@@ -29,14 +29,17 @@
     return jnp.cos(angles), jnp.sin(angles)
 
 
-def dispatch_kernel(experts, room, at_ref, tokens_ref, gain_ref, routes_ref, out_ref, where_ref):
+def dispatch_kernel(
+    experts, room, at_ref, tokens_ref, gain_ref, routes_ref, out_ref, where_ref, row_ref
+):
     rows, width = tokens_ref.shape
     share, pitch = out_ref.shape[2], 16 * (-(-room // 16))
     wide = tokens_ref[...].astype(F32)
     mean = jnp.sum(wide * wide, axis=-1, keepdims=True) * (1.0 / width)
     start = pl.multiple_of(at_ref[0] * share, share)
+    row_ref[...] = gain_ref[...].astype(F32)[None, :]
     mine = tokens_ref[:, pl.ds(start, share)].astype(F32) * lax.rsqrt(mean + EPSILON)
-    normed = (mine * gain_ref[:, pl.ds(start, share)].astype(F32)).astype(BF16)
+    normed = (mine * row_ref[:, pl.ds(start, share)]).astype(BF16)
     names = lax.broadcasted_iota(jnp.int32, (experts, rows), 0)
     first, second = routes_ref[0:1, :], routes_ref[1:2, :]
     hit_first = jnp.where(names == first, 1.0, 0.0)
@@ -69,32 +72,47 @@
         ),
         in_specs=[pl.BlockSpec(memory_space=pltpu.SMEM), vmem, vmem, vmem],
         out_specs=(vmem, vmem),
+        scratch_shapes=[pltpu.VMEM((1, tokens.shape[1]), F32)],
         compiler_params=params(60),
         cost_estimate=pl.CostEstimate(flops=10_000_000, bytes_accessed=700_000, transcendentals=0),
         name="dispatch",
-    )(at, tokens, gain.reshape(1, -1), routes.T)
-
-
-def expert_kernel(x_ref, gate_hbm, up_hbm, down_hbm, out_ref, gate_ref, up_ref, down_ref, sems):
+    )(at, tokens, gain, routes.T)
+
+
+def expert_kernel(x_hbm, gate_hbm, up_hbm, down_hbm, out_ref, x_ref, gate_ref, up_ref, down_ref, gate_acc, up_acc, sems):
     pieces, rows, share = x_ref.shape
-    loads = [
-        pltpu.make_async_copy(source, target, sems.at[n])
-        for n, (source, target) in enumerate(
-            ((gate_hbm, gate_ref), (up_hbm, up_ref), (down_hbm, down_ref))
-        )
-    ]
+    step, few = 128, pieces // 4
+    loads = []
+    for n in range(4):
+        some, deep = pl.ds(n * few, few), pl.ds(n * few * share, few * share)
+        for m, (source, target, part) in enumerate(
+            ((x_hbm, x_ref, some), (gate_hbm, gate_ref, deep), (up_hbm, up_ref, deep))
+        ):
+            loads.append(
+                pltpu.make_async_copy(source.at[part], target.at[part], sems.at[3 * n + m])
+            )
+    loads.append(pltpu.make_async_copy(down_hbm, down_ref, sems.at[12]))
     for load in loads:
         load.start()
-    loads[0].wait()
-    loads[1].wait()
-    step = 128
+    for n in range(4):
+        for load in loads[3 * n : 3 * n + 3]:
+            load.wait()
+        deep = pl.ds(n * few * share, few * share)
+        for at in range(0, rows, step):
+            x = jnp.concatenate(
+                [x_ref[n * few + p, at : at + step, :] for p in range(few)], axis=1
+            )
+            gate = jnp.dot(x, gate_ref[deep, :], preferred_element_type=F32)
+            up = jnp.dot(x, up_ref[deep, :], preferred_element_type=F32)
+            if n:
+                gate = gate + gate_acc[at : at + step, :]
+                up = up + up_acc[at : at + step, :]
+            gate_acc[at : at + step, :] = gate
+            up_acc[at : at + step, :] = up
+    loads[12].wait()
     for at in range(0, rows, step):
-        x = jnp.concatenate([x_ref[p, at : at + step, :] for p in range(pieces)], axis=1)
-        gate = jnp.dot(x, gate_ref[...], preferred_element_type=F32)
-        up = jnp.dot(x, up_ref[...], preferred_element_type=F32)
+        gate, up = gate_acc[at : at + step, :], up_acc[at : at + step, :]
         hidden = (gate / (1.0 + jnp.exp(-gate)) * up).astype(BF16)
-        if at == 0:
-            loads[2].wait()
         for p in range(0, pieces, 2):
             term = jnp.dot(
                 hidden, down_ref[:, p * share : (p + 2) * share], preferred_element_type=F32
@@ -104,15 +122,16 @@
 
 
 def expert(x, gate, up, down):
-    vmem = pl.BlockSpec(memory_space=pltpu.VMEM)
+    anywhere = pl.BlockSpec(memory_space=pl.ANY)
     return pl.pallas_call(
         expert_kernel,
         out_shape=jax.ShapeDtypeStruct(x.shape, BF16),
-        in_specs=[vmem] + [pl.BlockSpec(memory_space=pl.ANY)] * 3,
-        out_specs=vmem,
-        scratch_shapes=[pltpu.VMEM(w.shape, BF16) for w in (gate, up, down)]
-        + [pltpu.SemaphoreType.DMA((3,))],
-        compiler_params=params(56),
+        in_specs=[anywhere] * 4,
+        out_specs=pl.BlockSpec(memory_space=pltpu.VMEM),
+        scratch_shapes=[pltpu.VMEM(w.shape, BF16) for w in (x, gate, up, down)]
+        + [pltpu.VMEM((x.shape[1], gate.shape[1]), F32)] * 2
+        + [pltpu.SemaphoreType.DMA((13,))],
+        compiler_params=params(60),
         cost_estimate=pl.CostEstimate(flops=40_000_000, bytes_accessed=6_000_000, transcendentals=0),
         name="expert",
     )(x, gate, up, down)
@@ -152,7 +171,7 @@
 def normed_rows(ref, gain_ref):
     wide = ref[...].astype(F32)
     mean = jnp.sum(wide * wide, axis=-1, keepdims=True) * (1.0 / ref.shape[1])
-    return (wide * lax.rsqrt(mean + EPSILON) * gain_ref[...].astype(F32)).astype(BF16)
+    return (wide * lax.rsqrt(mean + EPSILON) * gain_ref[...].astype(F32)[None, :]).astype(BF16)
 
 
 def across(left, right):
@@ -185,7 +204,7 @@
         compiler_params=params(60),
         cost_estimate=pl.CostEstimate(flops=10_000_000, bytes_accessed=500_000, transcendentals=0),
         name="keys",
-    )(kv, gain.reshape(1, -1), rope_key.T, w_key.T, w_value.T, cosine, sine)
+    )(kv, gain, rope_key.T, w_key.T, w_value.T, cosine, sine)
 
 
 def queries_kernel(side, q_ref, gain_ref, nope_ref, rope_ref, cos_ref, sin_ref, out_ref):
@@ -212,24 +231,24 @@
         compiler_params=params(60),
         cost_estimate=pl.CostEstimate(flops=10_000_000, bytes_accessed=700_000, transcendentals=0),
         name="queries",
-    )(q_latent, gain.reshape(1, -1), w_nope.T, w_rope.T, cosine, sine)
-
-
-def attention_kernel(q_ref, own_ref, other_ref, out_ref, s_ref, acc_ref):
+    )(q_latent, gain, w_nope.T, w_rope.T, cosine, sine)
+
+
+def attention_kernel(q_ref, kv_ref, out_ref, s_ref, acc_ref):
     tile = 256
-    blocks, _, span = own_ref.shape
+    blocks, span = kv_ref.shape[0] // 2, kv_ref.shape[2]
     queries = q_ref.shape[1]
     cut = NOPE + ROPE
     rate = (NOPE + ROPE) ** (-0.5) * math.log2(math.e)
     pad = jnp.zeros((q_ref.shape[0] - cut, tile), BF16)
     ones = jnp.ones((16, tile), BF16)
-    tiles = [(ref, at) for ref in (own_ref, other_ref) for at in range(0, span, tile)]
+    tiles = [(part, at) for part in (0, 1) for at in range(0, span, tile)]
     halves = range(0, queries, tile)
 
     def score(block, slot, top):
         tops = [None for _ in halves]
-        for n, (ref, at) in enumerate(tiles):
-            keys = jnp.concatenate([ref[block, :cut, at : at + tile], pad], axis=0).T
+        for n, (part, at) in enumerate(tiles):
+            keys = jnp.concatenate([kv_ref[2 * block + part, :cut, at : at + tile], pad], axis=0).T
             for i, h in enumerate(halves):
                 s = jnp.dot(keys, q_ref[:, h : h + tile], preferred_element_type=F32)
                 s_ref[slot, n * tile : (n + 1) * tile, h : h + tile] = s
@@ -242,10 +261,10 @@
         shrink = jnp.exp2((old_top - top) * rate)
         for h in halves:
             total = acc_ref[:, h : h + tile] * shrink[:, h : h + tile]
-            for n, (ref, at) in enumerate(tiles):
+            for n, (part, at) in enumerate(tiles):
                 s = s_ref[slot, n * tile : (n + 1) * tile, h : h + tile]
                 weights = jnp.exp2((s - top[:, h : h + tile]) * rate).astype(BF16)
-                rows = jnp.concatenate([ref[block, cut:, at : at + tile], ones], axis=0)
+                rows = jnp.concatenate([kv_ref[2 * block + part, cut:, at : at + tile], ones], axis=0)
                 total = total + jnp.dot(rows, weights, preferred_element_type=F32)
             acc_ref[:, h : h + tile] = total
 
@@ -268,22 +287,22 @@
         out_ref[n] = done[:, n * out_ref.shape[2] : (n + 1) * out_ref.shape[2]]
 
 
-def attention(q, own, other, parts):
+def attention(q, kv, parts):
     vmem = pl.BlockSpec(memory_space=pltpu.VMEM)
     queries = q.shape[1]
     return pl.pallas_call(
         attention_kernel,
         out_shape=jax.ShapeDtypeStruct((parts, VDIM, queries // parts), BF16),
-        in_specs=[vmem] * 3,
+        in_specs=[vmem] * 2,
         out_specs=vmem,
         scratch_shapes=[
-            pltpu.VMEM((2, 2 * own.shape[2], queries), F32),
+            pltpu.VMEM((2, 2 * kv.shape[2], queries), F32),
             pltpu.VMEM((VDIM + 16, queries), F32),
         ],
         compiler_params=params(24),
         cost_estimate=pl.CostEstimate(flops=200_000_000, bytes_accessed=8_000_000, transcendentals=0),
         name="attention",
-    )(q, own, other)
+    )(q, kv)
 
 
 def ring(count, step):
@@ -301,6 +320,17 @@
     return [mine(0)] + [
         lax.ppermute(mine(k), axis, ring(count, k)) for k in range(1, count)
     ]
+
+
+def traded_in_two(pieces, axis):
+    count, me = lax.axis_size(axis), lax.axis_index(axis)
+    doubled = jnp.concatenate([pieces, pieces], axis=0)
+    turned_pieces = lax.dynamic_slice_in_dim(doubled, me, count, 0, allow_negative_indices=False)
+    far = lax.ppermute(turned_pieces[2:], axis, ring(count, 2))
+    near = lax.ppermute(
+        jnp.concatenate([turned_pieces[1:2], far[1:]], axis=0), axis, ring(count, 1)
+    )
+    return [turned_pieces[0], near[0], far[0], near[1]]
 
 
 def shards(
@@ -334,7 +364,7 @@
     mixed = places.reshape(side, side, -1).transpose(1, 0, 2).reshape(-1)
     cos_q, sin_q = turns(first_row + mixed, ROPE // 2)
     piece = keys(kv_latent, kv_gain, rope_key, w_k_nope, w_value, cos_k, sin_k)
-    own = lax.all_gather(piece, "z", axis=0, tiled=False)
+    gathered = lax.all_gather(piece, EP, axis=0, tiled=False)
     routes, piece = lax.optimization_barrier((routes, piece))
     outgoing, where = dispatch(
         tokens_b, norm_gain_b, routes, lax.axis_index(TP)[None], n_ep, room, share
@@ -347,9 +377,8 @@
     rows = lax.all_to_all(mine, TP, split_axis=0, concat_axis=0, tiled=True)
     terms = expert(rows, w_gate[0], w_up[0], w_down[0])
     terms = lax.all_to_all(terms, TP, split_axis=0, concat_axis=0, tiled=True)
-    other = lax.ppermute(own, "c", [(0, 1), (1, 0)])
-    heads = attention(q, own, other, side)
-    heads = jnp.concatenate(traded(heads, "x"), axis=0)
+    heads = attention(q, gathered, side)
+    heads = jnp.concatenate(traded_in_two(heads, "x"), axis=0)
     partial = lax.dot_general(
         heads, w_group, (((0,), (0,)), ((), ())), preferred_element_type=F32
     ).astype(BF16)

time: 182 us -> 153 us (0.84)
  blocking collectives: 33.4 us -> 60.8 us
  starting transfers between devices: 62.7 us -> 37.8 us
  waiting for transfers between devices: 33 us -> 9.79 us
  Pallas kernels: 25.3 us -> 21.9 us
  local copies, waits for them, and re-layouts: 7.82 us -> 4.77 us
    all_gather x1, waiting for transfers between devices: 29.2 us -> 0.01 us  [shards(): gathered = lax.all_gather(piece, EP, axis=0, tiled=False)]
    all_to_all x0 -> x1, blocking collectives: none -> 27.8 us  [shards(): rows = lax.all_to_all(mine, TP, split_axis=0, concat_axis=0, tiled=True)]
    ppermute x6 -> x3, starting transfers between devices: 18.9 us -> 9.93 us  [traded(): lax.ppermute(mine(k), axis, ring(count, k))]
    all_to_all x1 -> x0, starting transfers between devices: 6.9 us -> none  [shards(): rows = lax.all_to_all(mine, TP, split_axis=0, concat_axis=0, tiled=True)]
    ppermute x1 -> x2, starting transfers between devices: 10.1 us -> 3.85 us  [the longest x1 1.93 us: traded_in_two(): far = lax.ppermute(turned_pieces[2:], axis, ring(count, 2))]
    ppermute x1 -> x2, waiting for transfers between devices: 0.01 us -> 4.22 us  [the longest x1 4.21 us: traded_in_two(): far = lax.ppermute(turned_pieces[2:], axis, ring(count, 2))]
    all_to_all x1, starting transfers between devices: 7.01 us -> 3.86 us  [shards(): terms = lax.all_to_all(terms, TP, split_axis=0, concat_axis=0, tiled=True)]
    reshape x3 -> x0, local copies, waits for them, and re-layouts: 3.12 us -> none  [the longest x1 1.29 us: dispatch(): gain.reshape(1, -1)]
  transfers between devices with their start and end apart: 14 -> 11, of which waited for: 2 -> 2; matrix products, arithmetic and copies ran while one was open for 4% -> 1% of each run, Pallas kernels for 13% -> 13%
where the time goes in v2:
time: 153 us; the launch traced here: 152 us
  blocking collectives  60.8 us (40%)
  starting transfers between devices  37.8 us (25%)
  Pallas kernels  21.9 us (14%)
  between operations  14.3 us (9%)
  waiting for transfers between devices  9.79 us (6%)
  local copies, waits for them, and re-layouts  4.77 us (3%)
  other arithmetic  1.96 us (1%)
    all_to_all x1, blocking collectives, shards(): lax.all_to_all(outgoing, EP, split_axis=0, concat_axis=0, tiled=True)  32.9 us
    all_to_all x1, blocking collectives, shards(): rows = lax.all_to_all(mine, TP, split_axis=0, concat_axis=0, tiled=True)  27.8 us
    ppermute x3, starting transfers between devices, from_row(): lax.ppermute(value, axis, ring(count, k))  11.2 us
    pallas_call x1, Pallas kernels, attention(): pl.pallas_call(attention_kernel, out_shape=jax.ShapeDtypeStruct((parts, V...  10.2 us
    ppermute x3, starting transfers between devices, traded(): lax.ppermute(mine(k), axis, ring(count, k))  9.93 us
    all_to_all x1, starting transfers between devices, shards(): lax.all_to_all(finished.reshape(n_ep, room, share), EP, split_axis=0, con...  8.98 us
    all_to_all x1, waiting for transfers between devices, shards(): lax.all_to_all(finished.reshape(n_ep, room, share), EP, split_axis=0, con...  5.53 us
    pallas_call x1, Pallas kernels, expert(): pl.pallas_call(expert_kernel, out_shape=jax.ShapeDtypeStruct(x.shape, BF1...  4.25 us
  transfers between devices with their start and end apart: 11, of which 2 were waited for; matrix products, arithmetic and copies ran while one was open for 1% of the time, Pallas kernels for 13%

profile of v2, /device:TPU:1, one launch (start us, length us, event | category | flops | bytes accessed | tf_op | source)
XLA Modules:
  0.0 151.7 jit_solution(8569060258188323702)
XLA Ops:
  7.3 0.1 reshape.76
  7.3 0.9 multiply_sine_fusion
  8.3 2.0 %keys.1 = bf16[160,512]{1,0:T(8,128)(2,1)} custom-call(bf16[512,256]{1,0:T(8,128)(2,1)} %kv_ref.1, bf16[256]{0:T(256)(128)(2,1)} %gain_ref.1, bf16[32,512]{1,0:T(8,128)(2,1)} %bitcast.39, bf16[64,256]{1,0:T(8,128)(2,1)} %bitcast.40, bf16[64,256]{1,0:T(8,128)(2,1)} %bitcast.41, f32[16,512]{1,0:T(8,128)} %get-tuple-element.18.cos_ref, ...), custom_call_target="tpu_custom_call" | custom-call | flops 10000000 | bytes 500000 | tf_op jit(solution)/shard_map/keys/pallas_call | solution.py:199
  10.3 2.1 %dispatch.1 = (bf16[32,12,128]{2,1,0:T(8,128)(2,1)}, s32[2,128]{1,0:T(2,128)}) custom-call(s32[1]{0:T(128)} %bitcast.15.refs_0_, bf16[128,2048]{1,0:T(8,128)(2,1)} %refs_1_.3, bf16[2048]{0:T(1024)(128)(2,1)} %refs_2_.1, s32[2,128]{1,0:T(2,128)} %bitcast.42), custom_call_target="tpu_custom_call" | custom-call | flops 10000000 | bytes 700000 | tf_op jit(solution)/shard_map/dispatch/pallas_call | solution.py:67
  12.4 32.9 %all_to_all.20 = bf16[32,12,128]{2,1,0:T(8,128)(2,1)S(1)} all-to-all(bf16[32,12,128]{2,1,0:T(8,128)(2,1)} %get-tuple-element.6), channel_id=1, replica_groups=mesh['z'=16,'c'=2,'y'=4,'x'=4] {'z','c'}, dimensions={0} | all-to-all | bytes 196608 | tf_op jit(solution)/shard_map/all_to_all | solution.py:372
  45.4 0.3 broadcast_in_dim.16
  45.7 27.8 %all_to_all.21.x_hbm = bf16[16,384,128]{2,1,0:T(8,128)(2,1)} all-to-all(bf16[16,384,128]{2,1,0:T(8,128)(2,1)S(1)} %broadcast_in_dim.16), channel_id=1, replica_groups=mesh['z'=16,'c'=2,'y'=4,'x'=4] {'y','x'}, dimensions={0} | all-to-all | bytes 3145728 | tf_op jit(solution)/shard_map/all_to_all | solution.py:377
  73.6 4.2 %expert.1 = bf16[16,384,128]{2,1,0:T(8,128)(2,1)} custom-call(bf16[16,384,128]{2,1,0:T(8,128)(2,1)} %all_to_all.21.x_hbm, bf16[2048,256]{1,0:T(8,128)(2,1)} %bitcast.32, bf16[2048,256]{1,0:T(8,128)(2,1)} %bitcast.33, bf16[256,2048]{1,0:T(8,128)(2,1)} %bitcast.34), custom_call_target="tpu_custom_call" | custom-call | flops 40000000 | bytes 6000000 | tf_op jit(solution)/shard_map/expert/pallas_call | solution.py:126
  77.8 3.9 %all-to-all-start.2 = ((bf16[16,384,128]{2,1,0:T(8,128)(2,1)}), bf16[16,384,128]{2,1,0:T(8,128)(2,1)S(1)}, u32[]{:S(2)}, u32[]{:S(2)}) async-start(bf16[16,384,128]{2,1,0:T(8,128)(2,1)} %expert.1), calls=%async_computation.2 | async-start | bytes 3145728 | tf_op jit(solution)/shard_map/all_to_all | solution.py:379
  81.7 4.7 %collective-permute-start.3 = (bf16[64,2048]{1,0:T(8,128)(2,1)S(1)}, bf16[64,2048]{1,0:T(8,128)(2,1)S(1)}, u32[]{:S(2)}, u32[]{:S(2)}) collective-permute-start(bf16[64,2048]{1,0:T(8,128)(2,1)S(1)} %copy-done.4), channel_id=1, source_target_pairs={{0,2},{1,3},{2,0},{3,1},{4,6},{5,7},{6,4},{7,5},{8,10},{9,11},{10,... | collective-permute-start | bytes 786440 | tf_op jit(solution)/shard_map/ppermute | solution.py:314
  86.4 2.2 %collective-permute-start.2 = (bf16[64,2048]{1,0:T(8,128)(2,1)S(1)}, bf16[64,2048]{1,0:T(8,128)(2,1)S(1)}, u32[]{:S(2)}, u32[]{:S(2)}) collective-permute-start(bf16[64,2048]{1,0:T(8,128)(2,1)S(1)} %copy-done.4), channel_id=1, source_target_pairs={{0,1},{1,2},{2,3},{3,0},{4,5},{5,6},{6,7},{7,4},{8,9},{9,10},{10,1... | collective-permute-start | bytes 786440 | tf_op jit(solution)/shard_map/ppermute | solution.py:314
  88.6 4.3 %collective-permute-start.4 = (bf16[64,2048]{1,0:T(8,128)(2,1)S(1)}, bf16[64,2048]{1,0:T(8,128)(2,1)S(1)}, u32[]{:S(2)}, u32[]{:S(2)}) collective-permute-start(bf16[64,2048]{1,0:T(8,128)(2,1)S(1)} %copy-done.4), channel_id=1, source_target_pairs={{0,3},{1,0},{2,1},{3,2},{4,7},{5,4},{6,5},{7,6},{8,11},{9,8},{10,9... | collective-permute-start | bytes 786440 | tf_op jit(solution)/shard_map/ppermute | solution.py:314
  92.9 2.3 %queries.1.q_ref = bf16[128,512]{1,0:T(8,128)(2,1)} custom-call(bf16[512,512]{1,0:T(8,128)(2,1)} %refs_0_.1, bf16[512]{0:T(512)(128)(2,1)} %refs_1_.2, bf16[64,512]{1,0:T(8,128)(2,1)} %bitcast.37, bf16[32,512]{1,0:T(8,128)(2,1)} %bitcast.38, f32[16,512]{1,0:T(8,128)} %get-tuple-element.21.refs_4_, f32[16,512]{1,0:T(8,128)} %get-tuple-element.22.refs_5_), custom_call_target="tpu_custom_call" | custom-call | flops 10000000 | bytes 700000 | tf_op jit(solution)/shard_map/queries/pallas_call | solution.py:226
  95.2 2.5 %copy-done = bf16[5120,512]{1,0:T(8,128)(2,1)S(1)} copy-done((bf16[5120,512]{1,0:T(8,128)(2,1)S(1)}, bf16[5120,512]{1,0:T(8,128)(2,1)}, u32[]{:S(2)}) %copy-start) | copy-done | bytes 5242904
  97.7 0.9 copy-done.1
  98.6 10.2 %attention.1 = bf16[4,64,128]{2,1,0:T(8,128)(2,1)S(1)} custom-call(bf16[128,512]{1,0:T(8,128)(2,1)S(1)} %copy-done.1, bf16[32,160,512]{2,1,0:T(8,128)(2,1)S(1)} %bitcast.30), custom_call_target="tpu_custom_call" | custom-call | flops 200000000 | bytes 8000000 | tf_op jit(solution)/shard_map/attention/pallas_call | solution.py:293
  108.7 0.1 fusion.10
  108.8 1.9 %collective-permute-start = (bf16[2,64,128]{2,1,0:T(8,128)(2,1)S(1)}, bf16[2,64,128]{2,1,0:T(8,128)(2,1)S(1)}, u32[]{:S(2)}, u32[]{:S(2)}) collective-permute-start(bf16[2,64,128]{2,1,0:T(8,128)(2,1)S(1)} %slice.30), channel_id=1, source_target_pairs={{0,2},{1,3},{2,0},{3,1},{4,6},{5,7},{6,4},{7,5},{8,10},{9,11},{10,... | collective-permute-start | bytes 98312 | tf_op jit(solution)/shard_map/ppermute | solution.py:329
  110.8 4.2 %collective-permute-done = bf16[2,64,128]{2,1,0:T(8,128)(2,1)S(1)} collective-permute-done((bf16[2,64,128]{2,1,0:T(8,128)(2,1)S(1)}, bf16[2,64,128]{2,1,0:T(8,128)(2,1)S(1)}, u32[]{:S(2)}, u32[]{:S(2)}) %collective-permute-start) | collective-permute-done | bytes 32800 | tf_op jit(solution)/shard_map/ppermute | solution.py:329
  115.0 1.9 %collective-permute-start.1 = (bf16[2,64,128]{2,1,0:T(8,128)(2,1)S(1)}, bf16[2,64,128]{2,1,0:T(8,128)(2,1)S(1)}, u32[]{:S(2)}, u32[]{:S(2)}) collective-permute-start(bf16[2,64,128]{2,1,0:T(8,128)(2,1)S(1)} %pad_maximum_fusion), channel_id=1, source_target_pairs={{0,1},{1,2},{2,3},{3,0},{4,5},{5,6},{6,7},{7,4},{8,9},{9,10},{10,1... | collective-permute-start | bytes 98312 | tf_op jit(solution)/shard_map/ppermute | solution.py:330
  116.9 0.2 reduce_sum.12
  117.2 0.7 reshape.75
  117.8 9.0 %all-to-all-start.3 = ((bf16[32,12,128]{2,1,0:T(8,128)(2,1)}), bf16[32,12,128]{2,1,0:T(8,128)(2,1)S(1)}, u32[]{:S(2)}, u32[]{:S(2)}) async-start(bf16[32,12,128]{2,1,0:T(8,128)(2,1)} %reshape.75), calls=%async_computation.3 | async-start | bytes 262144 | tf_op jit(solution)/shard_map/all_to_all | solution.py:388
  126.9 0.3 convolution_convert_fusion
  127.3 3.1 %collective-permute-start.5 = (bf16[32,2048]{1,0:T(8,128)(2,1)S(1)}, bf16[32,2048]{1,0:T(8,128)(2,1)S(1)}, u32[]{:S(2)}, u32[]{:S(2)}) collective-permute-start(bf16[32,2048]{1,0:T(8,128)(2,1)S(1)} %get-tuple-element.8), channel_id=1, source_target_pairs={{0,4},{4,8},{8,12},{12,0},{1,5},{5,9},{9,13},{13,1},{2,6},{6,10},{... | collective-permute-start | bytes 393224 | tf_op jit(solution)/shard_map/ppermute | solution.py:321
  130.4 3.4 %collective-permute-start.7 = (bf16[32,2048]{1,0:T(8,128)(2,1)S(1)}, bf16[32,2048]{1,0:T(8,128)(2,1)S(1)}, u32[]{:S(2)}, u32[]{:S(2)}) collective-permute-start(bf16[32,2048]{1,0:T(8,128)(2,1)S(1)} %get-tuple-element.9), channel_id=1, source_target_pairs={{0,12},{4,0},{8,4},{12,8},{1,13},{5,1},{9,5},{13,9},{2,14},{6,2},{... | collective-permute-start | bytes 393224 | tf_op jit(solution)/shard_map/ppermute | solution.py:321
  133.8 3.4 %collective-permute-start.6 = (bf16[32,2048]{1,0:T(8,128)(2,1)S(1)}, bf16[32,2048]{1,0:T(8,128)(2,1)S(1)}, u32[]{:S(2)}, u32[]{:S(2)}) collective-permute-start(bf16[32,2048]{1,0:T(8,128)(2,1)S(1)} %get-tuple-element.10), channel_id=1, source_target_pairs={{0,8},{4,12},{8,0},{12,4},{1,9},{5,13},{9,1},{13,5},{2,10},{6,14},... | collective-permute-start | bytes 393224 | tf_op jit(solution)/shard_map/ppermute | solution.py:321
  137.3 0.1 copy.22.logits_ref
  137.4 0.1 copy.21
  137.5 5.5 %all-to-all-done.3.back_ref = bf16[32,12,128]{2,1,0:T(8,128)(2,1)S(1)} async-done(((bf16[32,12,128]{2,1,0:T(8,128)(2,1)}), bf16[32,12,128]{2,1,0:T(8,128)(2,1)S(1)}, u32[]{:S(2)}, u32[]{:S(2)}) %all-to-all-start.3) | async-done | bytes 98336 | tf_op jit(solution)/shard_map/all_to_all | solution.py:388
  143.0 1.0 combine.1
  144.1 0.7 fusion.9
  (29 shorter events, 0.2 us)
Async XLA Ops:
  7.2 88.0 %all-gather.3.cloned.1.call-start = ((), (), s32[]{:S(2)}) async-start(), calls=%async_computation.4 | async-start | bytes 5406720 | tf_op jit(solution)/shard_map/all_gather | solution.py:367
  77.8 3.9 %copy-start.4 = (bf16[64,2048]{1,0:T(8,128)(2,1)S(1)}, bf16[64,2048]{1,0:T(8,128)(2,1)}, u32[]{:S(2)}) copy-start(bf16[64,2048]{1,0:T(8,128)(2,1)} %param.26) | copy-start | bytes 786436
  77.8 39.1 %all-to-all-start.2 = ((bf16[16,384,128]{2,1,0:T(8,128)(2,1)}), bf16[16,384,128]{2,1,0:T(8,128)(2,1)S(1)}, u32[]{:S(2)}, u32[]{:S(2)}) async-start(bf16[16,384,128]{2,1,0:T(8,128)(2,1)} %expert.1), calls=%async_computation.2 | async-start | bytes 3145728 | tf_op jit(solution)/shard_map/all_to_all | solution.py:379
  81.7 45.1 %collective-permute-start.3 = (bf16[64,2048]{1,0:T(8,128)(2,1)S(1)}, bf16[64,2048]{1,0:T(8,128)(2,1)S(1)}, u32[]{:S(2)}, u32[]{:S(2)}) collective-permute-start(bf16[64,2048]{1,0:T(8,128)(2,1)S(1)} %copy-done.4), channel_id=1, source_target_pairs={{0,2},{1,3},{2,0},{3,1},{4,6},{5,7},{6,4},{7,5},{8,10},{9,11},{10,... | collective-permute-start | bytes 786440 | tf_op jit(solution)/shard_map/ppermute | solution.py:314
  86.4 40.5 %collective-permute-start.2 = (bf16[64,2048]{1,0:T(8,128)(2,1)S(1)}, bf16[64,2048]{1,0:T(8,128)(2,1)S(1)}, u32[]{:S(2)}, u32[]{:S(2)}) collective-permute-start(bf16[64,2048]{1,0:T(8,128)(2,1)S(1)} %copy-done.4), channel_id=1, source_target_pairs={{0,1},{1,2},{2,3},{3,0},{4,5},{5,6},{6,7},{7,4},{8,9},{9,10},{10,1... | collective-permute-start | bytes 786440 | tf_op jit(solution)/shard_map/ppermute | solution.py:314
  88.6 38.3 %collective-permute-start.4 = (bf16[64,2048]{1,0:T(8,128)(2,1)S(1)}, bf16[64,2048]{1,0:T(8,128)(2,1)S(1)}, u32[]{:S(2)}, u32[]{:S(2)}) collective-permute-start(bf16[64,2048]{1,0:T(8,128)(2,1)S(1)} %copy-done.4), channel_id=1, source_target_pairs={{0,3},{1,0},{2,1},{3,2},{4,7},{5,4},{6,5},{7,6},{8,11},{9,8},{10,9... | collective-permute-start | bytes 786440 | tf_op jit(solution)/shard_map/ppermute | solution.py:314
  95.2 2.5 %copy-start = (bf16[5120,512]{1,0:T(8,128)(2,1)S(1)}, bf16[5120,512]{1,0:T(8,128)(2,1)}, u32[]{:S(2)}) copy-start(bf16[5120,512]{1,0:T(8,128)(2,1)} %all-gather.3.cloned.1.call-done) | copy-start | bytes 15728644
  97.7 0.9 copy-start.1
  108.8 6.2 %collective-permute-start = (bf16[2,64,128]{2,1,0:T(8,128)(2,1)S(1)}, bf16[2,64,128]{2,1,0:T(8,128)(2,1)S(1)}, u32[]{:S(2)}, u32[]{:S(2)}) collective-permute-start(bf16[2,64,128]{2,1,0:T(8,128)(2,1)S(1)} %slice.30), channel_id=1, source_target_pairs={{0,2},{1,3},{2,0},{3,1},{4,6},{5,7},{6,4},{7,5},{8,10},{9,11},{10,... | collective-permute-start | bytes 98312 | tf_op jit(solution)/shard_map/ppermute | solution.py:329
  115.0 11.8 %collective-permute-start.1 = (bf16[2,64,128]{2,1,0:T(8,128)(2,1)S(1)}, bf16[2,64,128]{2,1,0:T(8,128)(2,1)S(1)}, u32[]{:S(2)}, u32[]{:S(2)}) collective-permute-start(bf16[2,64,128]{2,1,0:T(8,128)(2,1)S(1)} %pad_maximum_fusion), channel_id=1, source_target_pairs={{0,1},{1,2},{2,3},{3,0},{4,5},{5,6},{6,7},{7,4},{8,9},{9,10},{10,1... | collective-permute-start | bytes 98312 | tf_op jit(solution)/shard_map/ppermute | solution.py:330
  117.8 25.2 %all-to-all-start.3 = ((bf16[32,12,128]{2,1,0:T(8,128)(2,1)}), bf16[32,12,128]{2,1,0:T(8,128)(2,1)S(1)}, u32[]{:S(2)}, u32[]{:S(2)}) async-start(bf16[32,12,128]{2,1,0:T(8,128)(2,1)} %reshape.75), calls=%async_computation.3 | async-start | bytes 262144 | tf_op jit(solution)/shard_map/all_to_all | solution.py:388
  126.9 10.4 %copy-start.2 = (f32[128,2]{0,1:T(2,128)S(1)}, f32[128,2]{0,1:T(2,128)}, u32[]{:S(2)}) copy-start(f32[128,2]{0,1:T(2,128)} %param.30) | copy-start | bytes 3076
  126.9 10.5 %copy-start.3 = (s32[2,128]{1,0:T(2,128)S(1)}, s32[2,128]{1,0:T(2,128)}, u32[]{:S(2)}) copy-start(s32[2,128]{1,0:T(2,128)} %get-tuple-element.7) | copy-start | bytes 3076
  127.3 16.8 %collective-permute-start.5 = (bf16[32,2048]{1,0:T(8,128)(2,1)S(1)}, bf16[32,2048]{1,0:T(8,128)(2,1)S(1)}, u32[]{:S(2)}, u32[]{:S(2)}) collective-permute-start(bf16[32,2048]{1,0:T(8,128)(2,1)S(1)} %get-tuple-element.8), channel_id=1, source_target_pairs={{0,4},{4,8},{8,12},{12,0},{1,5},{5,9},{9,13},{13,1},{2,6},{6,10},{... | collective-permute-start | bytes 393224 | tf_op jit(solution)/shard_map/ppermute | solution.py:321
  130.4 13.7 %collective-permute-start.7 = (bf16[32,2048]{1,0:T(8,128)(2,1)S(1)}, bf16[32,2048]{1,0:T(8,128)(2,1)S(1)}, u32[]{:S(2)}, u32[]{:S(2)}) collective-permute-start(bf16[32,2048]{1,0:T(8,128)(2,1)S(1)} %get-tuple-element.9), channel_id=1, source_target_pairs={{0,12},{4,0},{8,4},{12,8},{1,13},{5,1},{9,5},{13,9},{2,14},{6,2},{... | collective-permute-start | bytes 393224 | tf_op jit(solution)/shard_map/ppermute | solution.py:321
  133.8 10.3 %collective-permute-start.6 = (bf16[32,2048]{1,0:T(8,128)(2,1)S(1)}, bf16[32,2048]{1,0:T(8,128)(2,1)S(1)}, u32[]{:S(2)}, u32[]{:S(2)}) collective-permute-start(bf16[32,2048]{1,0:T(8,128)(2,1)S(1)} %get-tuple-element.10), channel_id=1, source_target_pairs={{0,8},{4,12},{8,0},{12,4},{1,9},{5,13},{9,1},{13,5},{2,10},{6,14},... | collective-permute-start | bytes 393224 | tf_op jit(solution)/shard_map/ppermute | solution.py:321
Sparse Core Ops, SparseCore 0:
  10.5 81.9 all-gather.2
